TPU v7x, 256 devices: a whole 4x4x8 slice. The times are simulated.
256 devices in a mesh: sp: 64 (over z, y, core), tp: 4 (over x).
Axes of the slice: x: 4, y: 4, z: 8, core: 2. Of those that a mesh axis runs over, the one named last changes fastest.
Arguments:
- tokens: bfloat16 [4, 24576, 2048], P(None, 'sp'), may hold values from -21 to 21
- query_weight: bfloat16 [2048, 1024], P(None, 'tp'), may hold values from -0.125 to 0.125
- key_weight: bfloat16 [2048, 1024], P(None, 'tp'), may hold values from -0.125 to 0.125
- value_weight: bfloat16 [2048, 1024], P(None, 'tp'), may hold values from -0.125 to 0.125
- out_gain: float32 [1024], replicated, may hold values from 0.1 to 1.9
- out_weight: bfloat16 [1024, 2048], P(None, 'tp'), may hold values from -0.1875 to 0.1875
Outputs:
- mixed_out: bfloat16 [4, 24576, 2048], P(None, 'sp', 'tp')
- total_log: float32 [4, 8, 24576], P(None, 'tp', 'sp')
All inputs are finite; a program needn't handle non-finite values.
Results may differ from a plain program's by a relative error of at most 0.0098.
Values may be sent and summed in bfloat16 or wider, within the bound.
A program may use at most 128 MiB of HBM per device.

v0:
```python
import functools

import jax
import jax.numpy as jnp
from jax import lax
from jax.experimental import pallas as pl
from jax.experimental.pallas import tpu as pltpu
from jax.sharding import PartitionSpec as P

HEAD_DIM = 128
REACH = 64
ROPE_BASE = 10000.0
MASK_FILL = -1e30
NORM_FLOOR = 1e-6
LOG2E = 1.4426950408889634
SCALE = HEAD_DIM ** (-0.5)
RATE = SCALE * LOG2E

TOK = 384
CHIP = 2 * TOK
BLK = 256
WIDE = 1024
HALO = WIDE // BLK
OWN = CHIP // BLK
NBLK = 2 * HALO + OWN
ROWS = NBLK * BLK
MESH = pl.DeviceIdType.MESH
F32 = jnp.float32
BF16 = jnp.bfloat16


def dot_nt(a, b):
    return lax.dot_general(a, b, (((1,), (1,)), ((), ())), preferred_element_type=F32)


def dot(a, b):
    return jnp.dot(a, b, preferred_element_type=F32)


def attend(queries, keys, values, bias):
    scores = dot_nt(queries, keys) + bias
    peak = jnp.max(scores, axis=-1, keepdims=True)
    probs = jnp.exp2((scores - peak) * RATE)
    total = jnp.sum(probs, axis=-1, keepdims=True)
    return dot(probs.astype(BF16), values), peak, total


def iota(shape, dim):
    return lax.broadcasted_iota(jnp.int32, shape, dim)


def kernel(chips, tps, seqs, tokens, wq, wk, wv, gain, wo, cos, sin, out, logs,
           tok_v, wq_v, wk_v, wv_v, wo_v, kvown, qown, kvbuf, qbuf, kvp, qp, perm,
           bias1, bias4, bias16, acc1, peak1, sum1, mperm, lperm, mnat, lnat, lrx, mg, out_v,
           in_sem, loc_sem, kv_send, kv_recv, x_send, x_recv, l_send, l_recv, x_loc, out_sem):
    sp, tp = lax.axis_index("sp"), lax.axis_index("tp")
    chip, core = sp // 2, sp % 2

    loads = [pltpu.make_async_copy(wk, wk_v, in_sem.at[0]),
             pltpu.make_async_copy(tokens.at[0], tok_v.at[0], in_sem.at[4]),
             pltpu.make_async_copy(wv, wv_v, in_sem.at[1]),
             pltpu.make_async_copy(wq, wq_v, in_sem.at[2])]
    for s in range(1, seqs):
        loads.append(pltpu.make_async_copy(tokens.at[s], tok_v.at[s], in_sem.at[4 + s]))
    loads.append(pltpu.make_async_copy(wo, wo_v, in_sem.at[3]))
    for load in loads:
        load.start()

    barrier = pltpu.get_barrier_semaphore()
    partners = [(2 * chip + 1 - core, tp)]
    for step in (1, -1, 2, -2):
        for c in range(2):
            partners.append((2 * ((chip + chips + step) % chips) + c, tp))
    for dx in range(1, tps):
        for c in range(2):
            partners.append((2 * chip + c, (tp + dx) % tps))
    for partner in partners:
        pl.semaphore_signal(barrier, inc=1, device_id=partner, device_id_type=MESH)

    def row_of(at, size):
        return pl.ds(pl.multiple_of(at, 128), size)

    def remote(src, dst, send, recv, device):
        return pltpu.make_async_remote_copy(src_ref=src, dst_ref=dst, send_sem=send, recv_sem=recv,
                                            device_id=device, device_id_type=MESH)

    def kv_sends(s):
        after, before = (chip + 1) % chips, (chip + chips - 1) % chips
        far = (chip + chips + 4 * core - 2) % chips
        copies = []
        for h in range(2):
            copies.append(remote(kvown.at[s, h], kvbuf.at[s, row_of(BLK + TOK * core, TOK)],
                                 kv_send.at[s, h], kv_recv.at[s, 1 + core], (2 * after + h, tp)))
            copies.append(remote(kvown.at[s, h], kvbuf.at[s, row_of(WIDE + CHIP + TOK * core, TOK)],
                                 kv_send.at[s, 2 + h], kv_recv.at[s, 3 + core], (2 * before + h, tp)))
        for h in range(2):
            copies.append(remote(kvown.at[s, h, row_of(128 * core, BLK)],
                                 kvbuf.at[s, row_of((ROWS - BLK) * (1 - core), BLK)],
                                 kv_send.at[s, 4 + h], kv_recv.at[s, 6 - core], (2 * far + h, tp)))
        copies.append(remote(kvown.at[s, 1 - core], kvbuf.at[s, row_of(WIDE + TOK * core, TOK)],
                             kv_send.at[s, 6], kv_recv.at[s, 0], (2 * chip + 1 - core, tp)))
        return copies

    def q_send(s):
        return remote(qown.at[s, 1 - core], qbuf.at[s, row_of(TOK * core, TOK)],
                      kv_send.at[s, 7], kv_recv.at[s, 7], (2 * chip + 1 - core, tp))

    def local_copies(s):
        return [pltpu.make_async_copy(kvown.at[s, core], kvbuf.at[s, row_of(WIDE + TOK * core, TOK)], loc_sem.at[s, 0]),
                pltpu.make_async_copy(qown.at[s, core], qbuf.at[s, row_of(TOK * core, TOK)], loc_sem.at[s, 1])]

    def kv_arrivals(s):
        starts = [(WIDE + TOK * (1 - core), TOK), (BLK, TOK), (BLK + TOK, TOK),
                  (WIDE + CHIP, TOK), (WIDE + CHIP + TOK, TOK), (0, BLK), (ROWS - BLK, BLK)]
        waits = [remote(kvown.at[s, 0, pl.ds(0, size)], kvbuf.at[s, row_of(at, size)], kv_send.at[s, 0],
                        kv_recv.at[s, i], (2 * chip + 1 - core, tp)) for i, (at, size) in enumerate(starts)]
        waits.append(remote(qown.at[s, 0], qbuf.at[s, row_of(TOK * (1 - core), TOK)], kv_send.at[s, 0],
                            kv_recv.at[s, 7], (2 * chip + 1 - core, tp)))
        return waits

    head = 2 * tp + core

    def column_of(h):
        return pl.ds(pl.multiple_of(h * HEAD_DIM, HEAD_DIM), HEAD_DIM)

    def x_sends(s):
        copies = []
        for dx in range(1, tps):
            for c in range(2):
                copies.append(remote(mnat.at[s, pl.ds(TOK * c, TOK)], mg.at[s, :, column_of(head)],
                                     x_send.at[s, 2 * dx + c], x_recv.at[s, head], (2 * chip + c, (tp + dx) % tps)))
        copies.append(remote(mnat.at[s, row_of(TOK * (1 - core), TOK)], mg.at[s, :, column_of(head)],
                             x_send.at[s, 0], x_recv.at[s, head], (2 * chip + 1 - core, tp)))
        copies.append(remote(lnat.at[s, 1 - core], lrx.at[s], l_send.at[s], l_recv.at[s], (2 * chip + 1 - core, tp)))
        return copies

    def x_local(s):
        return pltpu.make_async_copy(mnat.at[s, row_of(TOK * core, TOK)], mg.at[s, :, column_of(head)], x_loc.at[s])

    def x_arrivals(s):
        waits = []
        for o in range(1, 2 * tps):
            other = (head + o) % (2 * tps)
            waits.append(remote(mnat.at[s, pl.ds(0, TOK)], mg.at[s, :, column_of(other)], x_send.at[s, 0],
                                x_recv.at[s, other], (2 * chip + 1 - core, tp)))
        waits.append(remote(lnat.at[s, 0], lrx.at[s], l_send.at[s], l_recv.at[s], (2 * chip + 1 - core, tp)))
        return waits

    row, col = iota((BLK, BLK), 0), iota((BLK, BLK), 1)
    perm[...] = jnp.where(col == (row % 16) * 16 + row // 16, 1.0, 0.0).astype(BF16)
    first = chip * CHIP
    limit = chips * CHIP
    for b in range(OWN):
        row, col = iota((BLK, BLK + 2 * REACH), 0), iota((BLK, BLK + 2 * REACH), 1)
        gap = (row % 16) * 16 + row // 16 - (col - REACH)
        at = first + b * BLK - REACH + col
        good = (gap >= -REACH) & (gap <= REACH) & (at >= 0) & (at < limit)
        bias1[b] = jnp.where(good, 0.0, MASK_FILL)
        row, col = iota((64, 192), 0), iota((64, 192), 1)
        gap = (row % 16) * 4 + row // 16 - ((col // 64 - 1) * 64 + (col % 16) * 4 + (col % 64) // 16)
        at = first + (b + col // 64 - 1) * BLK
        good = (gap >= -REACH) & (gap <= REACH) & (at >= 0) & (at < limit)
        bias4[b] = jnp.where(good, 0.0, MASK_FILL)
    row, col = iota((16 * OWN, 16 * NBLK), 0), iota((16 * OWN, 16 * NBLK), 1)
    gap = row - (col - 16 * HALO)
    at = first + (col // 16 - HALO) * BLK
    good = (gap >= -REACH) & (gap <= REACH) & (at >= 0) & (at < limit)
    bias16[...] = jnp.where(good, 0.0, MASK_FILL)

    def turned(x):
        return (x * cos[...] + pltpu.roll(x, HEAD_DIM // 2, 1) * sin[...]).astype(BF16)

    def project(s, _):
        pltpu.make_async_copy(tokens.at[s], tok_v.at[s], in_sem.at[4 + s]).wait()

        @pl.when(s == 0)
        def _():
            loads[0].wait()
        keys = dot(tok_v[s], wk_v[...])
        for h in range(2):
            kvown[s, h, :, :HEAD_DIM] = turned(keys[:, h * HEAD_DIM:(h + 1) * HEAD_DIM])

        @pl.when(s == 0)
        def _():
            loads[2].wait()
        values = dot(tok_v[s], wv_v[...])
        for h in range(2):
            kvown[s, h, :, HEAD_DIM:] = values[:, h * HEAD_DIM:(h + 1) * HEAD_DIM].astype(BF16)

        @pl.when(s == 0)
        def _():
            pl.semaphore_wait(barrier, len(partners))
        for copy in kv_sends(s):
            copy.start()
        local_copies(s)[0].start()

        @pl.when(s == 0)
        def _():
            loads[3].wait()
        queries = dot(tok_v[s], wq_v[...])
        for h in range(2):
            qown[s, h] = turned(queries[:, h * HEAD_DIM:(h + 1) * HEAD_DIM])
        q_send(s).start()
        local_copies(s)[1].start()
        return 0

    lax.fori_loop(0, seqs, project, 0)
    loads[-1].wait()

    def attention(s):
        for copy in local_copies(s):
            copy.wait()
        for copy in kv_arrivals(s):
            copy.wait_recv()

        def put_in_order(b, _):
            block = kvbuf[s, pl.ds(pl.multiple_of(b * BLK, BLK), BLK), :]
            kvp[b] = dot(perm[...], block).astype(BF16).reshape(4, 4, 16, 2 * HEAD_DIM)
            return 0
        lax.fori_loop(0, NBLK, put_in_order, 0)
        for b in range(OWN):
            block = dot(perm[...], qbuf[s, pl.ds(b * BLK, BLK), :]).astype(BF16)
            qp[b] = block.reshape(4, 4, 16, HEAD_DIM)
            near = pl.ds(WIDE + b * BLK - REACH, BLK + 2 * REACH)
            acc, peak, total = attend(block, kvbuf[s, near, :HEAD_DIM], kvbuf[s, near, HEAD_DIM:], bias1[b])
            acc1[b] = acc.reshape(4, 4, 16, HEAD_DIM)
            peak1[b] = jnp.broadcast_to(peak, (BLK, HEAD_DIM)).reshape(4, 4, 16, HEAD_DIM)
            sum1[b] = jnp.broadcast_to(total, (BLK, HEAD_DIM)).reshape(4, 4, 16, HEAD_DIM)

        def residue(r, _):
            middle = []
            for b in range(OWN):
                keys = kvp[b + HALO - 1:b + HALO + 2, :, r, :, :HEAD_DIM].reshape(192, HEAD_DIM)
                values = kvp[b + HALO - 1:b + HALO + 2, :, r, :, HEAD_DIM:].reshape(192, HEAD_DIM)
                middle.append(attend(qp[b, :, r].reshape(64, HEAD_DIM), keys, values, bias4[b]))
            for a in range(4):
                keys = kvp[:, a, r, :, :HEAD_DIM].reshape(16 * NBLK, HEAD_DIM)
                values = kvp[:, a, r, :, HEAD_DIM:].reshape(16 * NBLK, HEAD_DIM)
                wide = attend(qp[:, a, r].reshape(16 * OWN, HEAD_DIM), keys, values, bias16[...])
                for b in range(OWN):
                    near = (acc1[b, a, r], peak1[b, a, r], sum1[b, a, r])
                    mid = tuple(x[a * 16:(a + 1) * 16] for x in middle[b])
                    far = tuple(x[b * 16:(b + 1) * 16] for x in wide)
                    peak = jnp.maximum(jnp.maximum(near[1], mid[1]), far[1])
                    merged, total = 0.0, 0.0
                    for acc_g, peak_g, sum_g in (near, mid, far):
                        share = jnp.exp2((peak_g - peak) * RATE)
                        merged = merged + share * acc_g
                        total = total + share * sum_g
                    mperm[b, a, r] = (merged / total).astype(BF16)
                    lperm[b, a, r] = peak * SCALE + jnp.log(total)
            return 0
        lax.fori_loop(0, 4, residue, 0)
        for b in range(OWN):
            block = dot(perm[...], mperm[b].reshape(BLK, HEAD_DIM)).astype(BF16)
            mnat[s, pl.ds(b * BLK, BLK), :] = block
            column = lperm[b].reshape(BLK, HEAD_DIM)
            for half in range(2):
                hit = perm[:, half * 128:(half + 1) * 128].astype(F32)
                line = jnp.sum(jnp.where(hit > 0.5, column, 0.0), axis=0, keepdims=True)
                piece = 2 * b + half
                lnat[s, piece // 3, piece % 3:piece % 3 + 1, :] = line
        for copy in x_sends(s):
            copy.start()
        x_local(s).start()

    def finish(s):
        x_local(s).wait()
        for copy in x_arrivals(s):
            copy.wait_recv()
        lifted = mg[s].astype(F32)
        square = jnp.mean(lifted * lifted, axis=-1, keepdims=True)
        scaled = (lifted * gain[...]).astype(BF16)
        projected = dot(scaled, wo_v[...])
        out_v[s] = (projected * lax.rsqrt(square + NORM_FLOOR)).astype(BF16)
        pltpu.make_async_copy(out_v.at[s], out.at[s], out_sem.at[s]).start()
        mine, theirs = lnat[s, core], lrx[s]
        upper = jnp.where(core == 0, mine, theirs)
        lower = jnp.where(core == 0, theirs, mine)
        for piece in range(3):
            lanes = pl.ds(piece * 128, 128)
            logs[s, 0:1, lanes] = upper[piece:piece + 1]
            logs[s, 1:2, lanes] = lower[piece:piece + 1]

    def stage(s, _):
        attention(s)

        @pl.when(s > 0)
        def _():
            finish(s - 1)
        return 0

    lax.fori_loop(0, seqs, stage, 0)
    finish(seqs - 1)

    def drain(s, _):
        for copy in kv_sends(s):
            copy.wait_send()
        q_send(s).wait_send()
        for copy in x_sends(s):
            copy.wait_send()
        pltpu.make_async_copy(out_v.at[s], out.at[s], out_sem.at[s]).wait()
        return 0
    lax.fori_loop(0, seqs, drain, 0)


def shards(chips, tps, tokens, query_weight, key_weight, value_weight, out_gain, out_weight):
    seqs, length, model_dim = tokens.shape
    channels, out_cols = out_weight.shape
    positions = lax.axis_index("sp") * length + jnp.arange(length, dtype=jnp.int32)
    half_dim = HEAD_DIM // 2
    frequency = ROPE_BASE ** (-jnp.arange(half_dim, dtype=F32) / half_dim)
    angles = positions.astype(F32)[:, None] * frequency[None, :]
    cosine, sine = jnp.cos(angles), jnp.sin(angles)
    cosine = jnp.concatenate([cosine, cosine], axis=1)
    sine = jnp.concatenate([-sine, sine], axis=1)
    any_spec = pl.BlockSpec(memory_space=pl.ANY)
    vmem = pl.BlockSpec(memory_space=pltpu.VMEM)
    dma = pltpu.SemaphoreType.DMA
    grid4 = (OWN, 4, 4, 16, HEAD_DIM)
    return pl.pallas_call(
        functools.partial(kernel, chips, tps, seqs),
        out_shape=(jax.ShapeDtypeStruct((seqs, length, out_cols), BF16),
                   jax.ShapeDtypeStruct((seqs, 2, length), F32)),
        in_specs=[any_spec, any_spec, any_spec, any_spec, vmem, any_spec, vmem, vmem],
        out_specs=(any_spec, vmem),
        scratch_shapes=[
            pltpu.VMEM((seqs, TOK, model_dim), BF16),
            pltpu.VMEM((model_dim, 256), BF16),
            pltpu.VMEM((model_dim, 256), BF16),
            pltpu.VMEM((model_dim, 256), BF16),
            pltpu.VMEM((channels, out_cols), BF16),
            pltpu.VMEM((seqs, 2, TOK, 256), BF16),
            pltpu.VMEM((seqs, 2, TOK, 128), BF16),
            pltpu.VMEM((seqs, ROWS, 256), BF16),
            pltpu.VMEM((seqs, CHIP, 128), BF16),
            pltpu.VMEM((NBLK, 4, 4, 16, 256), BF16),
            pltpu.VMEM(grid4, BF16),
            pltpu.VMEM((BLK, BLK), BF16),
            pltpu.VMEM((OWN, BLK, BLK + 2 * REACH), F32),
            pltpu.VMEM((OWN, 64, 192), F32),
            pltpu.VMEM((16 * OWN, 16 * NBLK), F32),
            pltpu.VMEM(grid4, F32),
            pltpu.VMEM(grid4, F32),
            pltpu.VMEM(grid4, F32),
            pltpu.VMEM(grid4, BF16),
            pltpu.VMEM(grid4, F32),
            pltpu.VMEM((seqs, CHIP, 128), BF16),
            pltpu.VMEM((seqs, 2, 3, 128), F32),
            pltpu.VMEM((seqs, 3, 128), F32),
            pltpu.VMEM((seqs, TOK, channels), BF16),
            pltpu.VMEM((seqs, TOK, out_cols), BF16),
            dma((4 + seqs,)),
            dma((seqs, 2)),
            dma((seqs, 8)),
            dma((seqs, 8)),
            dma((seqs, 8)),
            dma((seqs, 8)),
            dma((seqs,)),
            dma((seqs,)),
            dma((seqs,)),
            dma((seqs,)),
        ],
        compiler_params=pltpu.CompilerParams(
            collective_id=0, has_side_effects=True, vmem_limit_bytes=60 * 1024 * 1024
        ),
    )(tokens, query_weight, key_weight, value_weight, out_gain.reshape(1, channels), out_weight, cosine, sine)


def solution(mesh):
    return jax.shard_map(
        functools.partial(shards, mesh.shape["sp"] // 2, mesh.shape["tp"]),
        mesh=mesh,
        in_specs=(
            P(None, "sp", None),
            P(None, "tp"),
            P(None, "tp"),
            P(None, "tp"),
            P(),
            P(None, "tp"),
        ),
        out_specs=(P(None, "sp", "tp"), P(None, "tp", "sp")),
        check_vma=False,
    )
```

profile of v0, /device:TPU:1, one launch (start us, length us, event | category | flops | bytes accessed | tf_op | source)
XLA Modules:
  0.0 110.3 jit_solution(3235734696584925407)
XLA Ops:
  0.7 0.8 fusion
  1.4 0.9 pad_maximum_fusion
  2.3 104.7 %shard_map.77 = (bf16[4,384,512]{2,1,0:T(8,128)(2,1)}, f32[4,2,384]{2,1,0:T(2,128)}) custom-call(bf16[4,384,2048]{2,1,0:T(8,128)(2,1)} %tokens.1, bf16[2048,256]{1,0:T(8,128)(2,1)} %wq.1, bf16[2048,256]{1,0:T(8,128)(2,1)} %wk.1, bf16[2048,256]{1,0:T(8,128)(2,1)} %wv.1, f32[1,1024]{1,0:T(1,128)} %bitcast.1, bf16[1024,512]{1,0:T(8,128)(2,1)} %wo.1, ...), custom_call_target="tpu_custom_call" | custom-call | tf_op jit(solution)/shard_map/pallas_call | solution.py:321
  107.1 0.0 copy-start
  107.1 2.7 %copy.10 = bf16[4,384,512]{2,1,0:T(8,128)(2,1)} copy(bf16[4,384,512]{2,1,0:T(8,128)(2,1)} %get-tuple-element.9) | data formatting | bytes 3145728
  109.7 0.0 copy-done
  109.7 0.6 copy.11
  (2 shorter events, 0.0 us)
Async XLA Ops:
  107.1 2.7 %copy-start = (f32[4,2,384]{2,1,0:T(2,128)S(1)}, f32[4,2,384]{2,1,0:T(2,128)}, u32[]{:S(2)}) copy-start(f32[4,2,384]{2,1,0:T(2,128)} %get-tuple-element.10) | copy-start | bytes 36868
where the time goes:
time: 110 us
  Pallas kernels  105 us (95%)
  local copies, waits for them, and re-layouts  3.26 us (3%)
  other arithmetic  1.69 us (2%)
    pallas_call x1, Pallas kernels, shards(): pl.pallas_call(functools.partial(kernel, chips, tps, seqs), out_shape=(ja...  105 us
    unnamed x4, local copies, waits for them, and re-layouts  3.26 us

commit v1 on v0

--- a/solution.py
+++ b/solution.py
@@ -37,12 +37,29 @@
     return jnp.dot(a, b, preferred_element_type=F32)
 
 
-def attend(queries, keys, values, bias):
-    scores = dot_nt(queries, keys) + bias
+def softened(scores):
     peak = jnp.max(scores, axis=-1, keepdims=True)
     probs = jnp.exp2((scores - peak) * RATE)
-    total = jnp.sum(probs, axis=-1, keepdims=True)
-    return dot(probs.astype(BF16), values), peak, total
+    return probs.astype(BF16), peak, jnp.sum(probs, axis=-1, keepdims=True)
+
+
+def pipelined(jobs):
+    ahead = jobs[0][0]()
+    for i, (_, finish) in enumerate(jobs):
+        now = ahead
+        if i + 1 < len(jobs):
+            ahead = jobs[i + 1][0]()
+        finish(now)
+
+
+def joined(parts):
+    peak = functools.reduce(jnp.maximum, [part[1] for part in parts])
+    merged, total = 0.0, 0.0
+    for acc_g, peak_g, sum_g in parts:
+        share = jnp.exp2((peak_g - peak) * RATE)
+        merged = merged + share * acc_g
+        total = total + share * sum_g
+    return merged, peak, total
 
 
 def iota(shape, dim):
@@ -68,7 +85,7 @@
 
     barrier = pltpu.get_barrier_semaphore()
     partners = [(2 * chip + 1 - core, tp)]
-    for step in (1, -1, 2, -2):
+    for step in (1, -1):
         for c in range(2):
             partners.append((2 * ((chip + chips + step) % chips) + c, tp))
     for dx in range(1, tps):
@@ -84,39 +101,45 @@
         return pltpu.make_async_remote_copy(src_ref=src, dst_ref=dst, send_sem=send, recv_sem=recv,
                                             device_id=device, device_id_type=MESH)
 
-    def kv_sends(s):
-        after, before = (chip + 1) % chips, (chip + chips - 1) % chips
-        far = (chip + chips + 4 * core - 2) % chips
+    after, before = (chip + 1) % chips, (chip + chips - 1) % chips
+
+    def near_sends(s):
         copies = []
-        for h in range(2):
-            copies.append(remote(kvown.at[s, h], kvbuf.at[s, row_of(BLK + TOK * core, TOK)],
-                                 kv_send.at[s, h], kv_recv.at[s, 1 + core], (2 * after + h, tp)))
-            copies.append(remote(kvown.at[s, h], kvbuf.at[s, row_of(WIDE + CHIP + TOK * core, TOK)],
-                                 kv_send.at[s, 2 + h], kv_recv.at[s, 3 + core], (2 * before + h, tp)))
-        for h in range(2):
-            copies.append(remote(kvown.at[s, h, row_of(128 * core, BLK)],
-                                 kvbuf.at[s, row_of((ROWS - BLK) * (1 - core), BLK)],
-                                 kv_send.at[s, 4 + h], kv_recv.at[s, 6 - core], (2 * far + h, tp)))
-        copies.append(remote(kvown.at[s, 1 - core], kvbuf.at[s, row_of(WIDE + TOK * core, TOK)],
-                             kv_send.at[s, 6], kv_recv.at[s, 0], (2 * chip + 1 - core, tp)))
+        for piece, (src, at, size) in enumerate(((128 * core, 512 * core, BLK), (BLK * (1 - core), BLK + 128 * core, 128))):
+            for h in range(2):
+                for way, (base, to) in enumerate(((BLK, after), (WIDE + CHIP, before))):
+                    copies.append(remote(kvown.at[s, h, row_of(src, size)], kvbuf.at[s, row_of(base + at, size)],
+                                         kv_send.at[s, 4 * piece + 2 * h + way],
+                                         kv_recv.at[s, 4 * way + 2 * piece + core], (2 * to + h, tp)))
         return copies
 
-    def q_send(s):
-        return remote(qown.at[s, 1 - core], qbuf.at[s, row_of(TOK * core, TOK)],
-                      kv_send.at[s, 7], kv_recv.at[s, 7], (2 * chip + 1 - core, tp))
+    def far_sends(s):
+        return [remote(kvbuf.at[s, pl.ds(WIDE - BLK, BLK)], kvbuf.at[s, pl.ds(0, BLK)],
+                       kv_send.at[s, 8], kv_recv.at[s, 8], (2 * after + core, tp)),
+                remote(kvbuf.at[s, pl.ds(WIDE + CHIP, BLK)], kvbuf.at[s, pl.ds(ROWS - BLK, BLK)],
+                       kv_send.at[s, 9], kv_recv.at[s, 9], (2 * before + core, tp))]
+
+    def own_sends(s):
+        return [remote(kvown.at[s, 1 - core], kvbuf.at[s, row_of(WIDE + TOK * core, TOK)],
+                       kv_send.at[s, 10], kv_recv.at[s, 10], (2 * chip + 1 - core, tp)),
+                remote(qown.at[s, 1 - core], qbuf.at[s, row_of(TOK * core, TOK)],
+                       kv_send.at[s, 11], kv_recv.at[s, 11], (2 * chip + 1 - core, tp))]
 
     def local_copies(s):
         return [pltpu.make_async_copy(kvown.at[s, core], kvbuf.at[s, row_of(WIDE + TOK * core, TOK)], loc_sem.at[s, 0]),
                 pltpu.make_async_copy(qown.at[s, core], qbuf.at[s, row_of(TOK * core, TOK)], loc_sem.at[s, 1])]
 
-    def kv_arrivals(s):
-        starts = [(WIDE + TOK * (1 - core), TOK), (BLK, TOK), (BLK + TOK, TOK),
-                  (WIDE + CHIP, TOK), (WIDE + CHIP + TOK, TOK), (0, BLK), (ROWS - BLK, BLK)]
-        waits = [remote(kvown.at[s, 0, pl.ds(0, size)], kvbuf.at[s, row_of(at, size)], kv_send.at[s, 0],
-                        kv_recv.at[s, i], (2 * chip + 1 - core, tp)) for i, (at, size) in enumerate(starts)]
-        waits.append(remote(qown.at[s, 0], qbuf.at[s, row_of(TOK * (1 - core), TOK)], kv_send.at[s, 0],
-                            kv_recv.at[s, 7], (2 * chip + 1 - core, tp)))
-        return waits
+    def near_arrival(s, way, piece, c):
+        at, size = ((512 * c, BLK), (BLK + 128 * c, 128))[piece]
+        at += (BLK, WIDE + CHIP)[way]
+        return remote(kvown.at[s, 0, pl.ds(0, size)], kvbuf.at[s, pl.ds(at, size)], kv_send.at[s, 0],
+                      kv_recv.at[s, 4 * way + 2 * piece + c], (2 * chip + 1 - core, tp))
+
+    def own_arrivals(s):
+        return [remote(kvown.at[s, 0], kvbuf.at[s, row_of(WIDE + TOK * (1 - core), TOK)], kv_send.at[s, 0],
+                       kv_recv.at[s, 10], (2 * chip + 1 - core, tp)),
+                remote(qown.at[s, 0], qbuf.at[s, row_of(TOK * (1 - core), TOK)], kv_send.at[s, 0],
+                       kv_recv.at[s, 11], (2 * chip + 1 - core, tp))]
 
     head = 2 * tp + core
 
@@ -145,6 +168,47 @@
                                 x_recv.at[s, other], (2 * chip + 1 - core, tp)))
         waits.append(remote(lnat.at[s, 0], lrx.at[s], l_send.at[s], l_recv.at[s], (2 * chip + 1 - core, tp)))
         return waits
+
+    def turned(x):
+        return (x * cos[...] + pltpu.roll(x, HEAD_DIM // 2, 1) * sin[...]).astype(BF16)
+
+    def project(s, _):
+        pltpu.make_async_copy(tokens.at[s], tok_v.at[s], in_sem.at[4 + s]).wait()
+
+        @pl.when(s == 0)
+        def _():
+            loads[0].wait()
+        keys = dot(tok_v[s], wk_v[...])
+        for h in range(2):
+            kvown[s, h, :, :HEAD_DIM] = turned(keys[:, h * HEAD_DIM:(h + 1) * HEAD_DIM])
+
+        @pl.when(s == 0)
+        def _():
+            loads[2].wait()
+        values = dot(tok_v[s], wv_v[...])
+        for h in range(2):
+            kvown[s, h, :, HEAD_DIM:] = values[:, h * HEAD_DIM:(h + 1) * HEAD_DIM].astype(BF16)
+
+        @pl.when(s == 0)
+        def _():
+            pl.semaphore_wait(barrier, len(partners))
+            for copy in near_sends(0):
+                copy.start()
+        own_sends(s)[0].start()
+        local_copies(s)[0].start()
+
+        @pl.when(s == 0)
+        def _():
+            loads[3].wait()
+        queries = dot(tok_v[s], wq_v[...])
+        for h in range(2):
+            qown[s, h] = turned(queries[:, h * HEAD_DIM:(h + 1) * HEAD_DIM])
+        own_sends(s)[1].start()
+        local_copies(s)[1].start()
+        return 0
+
+    lax.fori_loop(0, seqs, project, 0)
+    loads[-1].wait()
 
     row, col = iota((BLK, BLK), 0), iota((BLK, BLK), 1)
     perm[...] = jnp.where(col == (row % 16) * 16 + row // 16, 1.0, 0.0).astype(BF16)
@@ -167,102 +231,99 @@
     good = (gap >= -REACH) & (gap <= REACH) & (at >= 0) & (at < limit)
     bias16[...] = jnp.where(good, 0.0, MASK_FILL)
 
-    def turned(x):
-        return (x * cos[...] + pltpu.roll(x, HEAD_DIM // 2, 1) * sin[...]).astype(BF16)
-
-    def project(s, _):
-        pltpu.make_async_copy(tokens.at[s], tok_v.at[s], in_sem.at[4 + s]).wait()
-
-        @pl.when(s == 0)
-        def _():
-            loads[0].wait()
-        keys = dot(tok_v[s], wk_v[...])
-        for h in range(2):
-            kvown[s, h, :, :HEAD_DIM] = turned(keys[:, h * HEAD_DIM:(h + 1) * HEAD_DIM])
-
-        @pl.when(s == 0)
-        def _():
-            loads[2].wait()
-        values = dot(tok_v[s], wv_v[...])
-        for h in range(2):
-            kvown[s, h, :, HEAD_DIM:] = values[:, h * HEAD_DIM:(h + 1) * HEAD_DIM].astype(BF16)
-
-        @pl.when(s == 0)
-        def _():
-            pl.semaphore_wait(barrier, len(partners))
-        for copy in kv_sends(s):
-            copy.start()
-        local_copies(s)[0].start()
-
-        @pl.when(s == 0)
-        def _():
-            loads[3].wait()
-        queries = dot(tok_v[s], wq_v[...])
-        for h in range(2):
-            qown[s, h] = turned(queries[:, h * HEAD_DIM:(h + 1) * HEAD_DIM])
-        q_send(s).start()
-        local_copies(s)[1].start()
-        return 0
-
-    lax.fori_loop(0, seqs, project, 0)
-    loads[-1].wait()
-
-    def attention(s):
-        for copy in local_copies(s):
-            copy.wait()
-        for copy in kv_arrivals(s):
-            copy.wait_recv()
-
-        def put_in_order(b, _):
-            block = kvbuf[s, pl.ds(pl.multiple_of(b * BLK, BLK), BLK), :]
-            kvp[b] = dot(perm[...], block).astype(BF16).reshape(4, 4, 16, 2 * HEAD_DIM)
-            return 0
-        lax.fori_loop(0, NBLK, put_in_order, 0)
+
+    def put_in_order(s, blocks):
+        for b in blocks:
+            kvp[b] = dot(perm[...], kvbuf[s, pl.ds(b * BLK, BLK), :]).astype(BF16).reshape(4, 4, 16, 2 * HEAD_DIM)
+
+    def near(s):
         for b in range(OWN):
             block = dot(perm[...], qbuf[s, pl.ds(b * BLK, BLK), :]).astype(BF16)
             qp[b] = block.reshape(4, 4, 16, HEAD_DIM)
-            near = pl.ds(WIDE + b * BLK - REACH, BLK + 2 * REACH)
-            acc, peak, total = attend(block, kvbuf[s, near, :HEAD_DIM], kvbuf[s, near, HEAD_DIM:], bias1[b])
-            acc1[b] = acc.reshape(4, 4, 16, HEAD_DIM)
-            peak1[b] = jnp.broadcast_to(peak, (BLK, HEAD_DIM)).reshape(4, 4, 16, HEAD_DIM)
-            sum1[b] = jnp.broadcast_to(total, (BLK, HEAD_DIM)).reshape(4, 4, 16, HEAD_DIM)
-
-        def residue(r, _):
-            middle = []
-            for b in range(OWN):
-                keys = kvp[b + HALO - 1:b + HALO + 2, :, r, :, :HEAD_DIM].reshape(192, HEAD_DIM)
-                values = kvp[b + HALO - 1:b + HALO + 2, :, r, :, HEAD_DIM:].reshape(192, HEAD_DIM)
-                middle.append(attend(qp[b, :, r].reshape(64, HEAD_DIM), keys, values, bias4[b]))
-            for a in range(4):
-                keys = kvp[:, a, r, :, :HEAD_DIM].reshape(16 * NBLK, HEAD_DIM)
-                values = kvp[:, a, r, :, HEAD_DIM:].reshape(16 * NBLK, HEAD_DIM)
-                wide = attend(qp[:, a, r].reshape(16 * OWN, HEAD_DIM), keys, values, bias16[...])
-                for b in range(OWN):
-                    near = (acc1[b, a, r], peak1[b, a, r], sum1[b, a, r])
-                    mid = tuple(x[a * 16:(a + 1) * 16] for x in middle[b])
-                    far = tuple(x[b * 16:(b + 1) * 16] for x in wide)
-                    peak = jnp.maximum(jnp.maximum(near[1], mid[1]), far[1])
-                    merged, total = 0.0, 0.0
-                    for acc_g, peak_g, sum_g in (near, mid, far):
-                        share = jnp.exp2((peak_g - peak) * RATE)
-                        merged = merged + share * acc_g
-                        total = total + share * sum_g
-                    mperm[b, a, r] = (merged / total).astype(BF16)
-                    lperm[b, a, r] = peak * SCALE + jnp.log(total)
-            return 0
-        lax.fori_loop(0, 4, residue, 0)
+        put_in_order(s, range(1, NBLK - 1))
+        jobs, done = [], {}
+
+        def narrow(b, half):
+            around = pl.ds(WIDE + b * BLK - REACH, BLK + 2 * REACH)
+
+            def scores():
+                queries = qp[b, 2 * half:2 * half + 2].reshape(128, HEAD_DIM)
+                return dot_nt(queries, kvbuf[s, around, :HEAD_DIM]) + bias1[b, half * 128:(half + 1) * 128]
+
+            def finish(scores):
+                probs, peak, total = softened(scores)
+                done[b, half] = dot(probs, kvbuf[s, around, HEAD_DIM:]), peak, total
+            return scores, finish
+
+        def middle(b):
+            def scores():
+                every = []
+                for r in range(4):
+                    keys = kvp[b + HALO - 1:b + HALO + 2, :, r, :, :HEAD_DIM].reshape(192, HEAD_DIM)
+                    every.append(dot_nt(qp[b, :, r].reshape(64, HEAD_DIM), keys) + bias4[b])
+                return every
+
+            def finish(every):
+                soft = [softened(scores) for scores in every]
+                accs = []
+                for r in range(4):
+                    values = kvp[b + HALO - 1:b + HALO + 2, :, r, :, HEAD_DIM:].reshape(192, HEAD_DIM)
+                    accs.append(dot(soft[r][0], values))
+                for a in range(4):
+                    for r in range(4):
+                        at = (a % 2) * 64 + r * 16
+                        one = tuple(x[at:at + 16] for x in done[b, a // 2])
+                        two = tuple(x[a * 16:(a + 1) * 16] for x in (accs[r],) + soft[r][1:])
+                        acc, peak, total = joined((one, two))
+                        acc1[b, a, r] = acc
+                        peak1[b, a, r] = jnp.broadcast_to(peak, (16, HEAD_DIM))
+                        sum1[b, a, r] = jnp.broadcast_to(total, (16, HEAD_DIM))
+            return scores, finish
+
         for b in range(OWN):
-            block = dot(perm[...], mperm[b].reshape(BLK, HEAD_DIM)).astype(BF16)
-            mnat[s, pl.ds(b * BLK, BLK), :] = block
+            jobs += [narrow(b, 0), narrow(b, 1), middle(b)]
+        pipelined(jobs)
+
+    def far(s):
+        put_in_order(s, (0, NBLK - 1))
+
+        def wide(r):
+            def scores():
+                every = []
+                for a in range(4):
+                    keys = kvp[:, a, r, :, :HEAD_DIM].reshape(16 * NBLK, HEAD_DIM)
+                    every.append(dot_nt(qp[:, a, r].reshape(16 * OWN, HEAD_DIM), keys) + bias16[...])
+                return every
+
+            def finish(every):
+                soft = [softened(scores) for scores in every]
+                accs = []
+                for a in range(4):
+                    values = kvp[:, a, r, :, HEAD_DIM:].reshape(16 * NBLK, HEAD_DIM)
+                    accs.append(dot(soft[a][0], values))
+                for a in range(4):
+                    for b in range(OWN):
+                        one = (acc1[b, a, r], peak1[b, a, r], sum1[b, a, r])
+                        two = tuple(x[b * 16:(b + 1) * 16] for x in (accs[a],) + soft[a][1:])
+                        merged, peak, total = joined((one, two))
+                        mperm[b, a, r] = (merged / total).astype(BF16)
+                        lperm[b, a, r] = peak * SCALE + jnp.log(total)
+            return scores, finish
+
+        pipelined([wide(r) for r in range(4)])
+        for b in range(OWN):
+            mnat[s, pl.ds(b * BLK, BLK), :] = dot(perm[...], mperm[b].reshape(BLK, HEAD_DIM)).astype(BF16)
+        for copy in x_sends(s)[:-1]:
+            copy.start()
+        x_local(s).start()
+        for b in range(OWN):
             column = lperm[b].reshape(BLK, HEAD_DIM)
             for half in range(2):
                 hit = perm[:, half * 128:(half + 1) * 128].astype(F32)
                 line = jnp.sum(jnp.where(hit > 0.5, column, 0.0), axis=0, keepdims=True)
                 piece = 2 * b + half
                 lnat[s, piece // 3, piece % 3:piece % 3 + 1, :] = line
-        for copy in x_sends(s):
-            copy.start()
-        x_local(s).start()
+        x_sends(s)[-1].start()
 
     def finish(s):
         x_local(s).wait()
@@ -283,7 +344,29 @@
             logs[s, 1:2, lanes] = lower[piece:piece + 1]
 
     def stage(s, _):
-        attention(s)
+        near_arrival(s, 0, 0, 1).wait_recv()
+        near_arrival(s, 1, 0, 0).wait_recv()
+        for copy in far_sends(s):
+            copy.start()
+
+        @pl.when(s + 1 < seqs)
+        def _():
+            for copy in near_sends(s + 1):
+                copy.start()
+
+        for copy in local_copies(s):
+            copy.wait()
+        for copy in own_arrivals(s):
+            copy.wait_recv()
+        near_arrival(s, 0, 0, 0).wait_recv()
+        near_arrival(s, 1, 0, 1).wait_recv()
+        for way in range(2):
+            for c in range(2):
+                near_arrival(s, way, 1, c).wait_recv()
+        near(s)
+        for copy in far_sends(s):
+            copy.wait_recv()
+        far(s)
 
         @pl.when(s > 0)
         def _():
@@ -294,9 +377,8 @@
     finish(seqs - 1)
 
     def drain(s, _):
-        for copy in kv_sends(s):
+        for copy in near_sends(s) + far_sends(s) + own_sends(s):
             copy.wait_send()
-        q_send(s).wait_send()
         for copy in x_sends(s):
             copy.wait_send()
         pltpu.make_async_copy(out_v.at[s], out.at[s], out_sem.at[s]).wait()
@@ -352,8 +434,8 @@
             pltpu.VMEM((seqs, TOK, out_cols), BF16),
             dma((4 + seqs,)),
             dma((seqs, 2)),
-            dma((seqs, 8)),
-            dma((seqs, 8)),
+            dma((seqs, 12)),
+            dma((seqs, 12)),
             dma((seqs, 8)),
             dma((seqs, 8)),
             dma((seqs,)),

time: 110 us -> 84.4 us (0.77)
  Pallas kernels: 105 us -> 78.6 us
    pallas_call x1, Pallas kernels: 105 us -> 78.6 us  [shards(): pl.pallas_call(functools.partial(kernel, chips, tps, seqs), out_shape=(ja...]
where the time goes in v1:
time: 84.4 us; the launch traced here: 84.2 us
  Pallas kernels  78.6 us (93%)
  local copies, waits for them, and re-layouts  3.26 us (4%)
  other arithmetic  1.69 us (2%)
    pallas_call x1, Pallas kernels, shards(): pl.pallas_call(functools.partial(kernel, chips, tps, seqs), out_shape=(ja...  78.6 us
    unnamed x4, local copies, waits for them, and re-layouts  3.26 us

profile of v1, /device:TPU:1, one launch (start us, length us, event | category | flops | bytes accessed | tf_op | source)
XLA Modules:
  0.0 84.2 jit_solution(4598812423376532936)
XLA Ops:
  0.7 0.8 fusion
  1.4 0.9 %pad_maximum_fusion = (f32[384,128]{1,0:T(8,128)}, f32[384,128]{1,0:T(8,128)}) fusion(f32[384,64]{1,0:T(8,128)S(1)} %get-tuple-element.4, f32[384,64]{1,0:T(8,128)S(1)} %get-tuple-element.3, f32[384,64]{1,0:T(8,128)S(1)} %get-tuple-element.2), kind=kLoop, calls=%fused_computation.2 | loop fusion | flops 98304 | bytes 688128 | tf_op jit(solution)/shard_map/concatenate | solution.py:397
  2.3 78.6 %shard_map.77 = (bf16[4,384,512]{2,1,0:T(8,128)(2,1)}, f32[4,2,384]{2,1,0:T(2,128)}) custom-call(bf16[4,384,2048]{2,1,0:T(8,128)(2,1)} %tokens.1, bf16[2048,256]{1,0:T(8,128)(2,1)} %wq.1, bf16[2048,256]{1,0:T(8,128)(2,1)} %wk.1, bf16[2048,256]{1,0:T(8,128)(2,1)} %wv.1, f32[1,1024]{1,0:T(1,128)} %bitcast.1, bf16[1024,512]{1,0:T(8,128)(2,1)} %wo.1, ...), custom_call_target="tpu_custom_call" | custom-call | tf_op jit(solution)/shard_map/pallas_call | solution.py:403
  81.0 0.0 copy-start
  81.0 2.7 %copy.10 = bf16[4,384,512]{2,1,0:T(8,128)(2,1)} copy(bf16[4,384,512]{2,1,0:T(8,128)(2,1)} %get-tuple-element.9) | data formatting | bytes 3145728
  83.6 0.0 copy-done
  83.6 0.6 copy.11
  (2 shorter events, 0.0 us)
Async XLA Ops:
  81.0 2.7 %copy-start = (f32[4,2,384]{2,1,0:T(2,128)S(1)}, f32[4,2,384]{2,1,0:T(2,128)}, u32[]{:S(2)}) copy-start(f32[4,2,384]{2,1,0:T(2,128)} %get-tuple-element.10) | copy-start | bytes 36868

commit v2 on v1

--- a/solution.py
+++ b/solution.py
@@ -66,8 +66,8 @@
     return lax.broadcasted_iota(jnp.int32, shape, dim)
 
 
-def kernel(chips, tps, seqs, tokens, wq, wk, wv, gain, wo, cos, sin, out, logs,
-           tok_v, wq_v, wk_v, wv_v, wo_v, kvown, qown, kvbuf, qbuf, kvp, qp, perm,
+def kernel(chips, tps, seqs, tokens, wq, wk, wv, gain, wo, frequency, out, logs,
+           cos, sin, tok_v, wq_v, wk_v, wv_v, wo_v, kvown, qown, kvbuf, qbuf, kvp, qp, perm,
            bias1, bias4, bias16, acc1, peak1, sum1, mperm, lperm, mnat, lnat, lrx, mg, out_v,
            in_sem, loc_sem, kv_send, kv_recv, x_send, x_recv, l_send, l_recv, x_loc, out_sem):
     sp, tp = lax.axis_index("sp"), lax.axis_index("tp")
@@ -85,14 +85,24 @@
 
     barrier = pltpu.get_barrier_semaphore()
     partners = [(2 * chip + 1 - core, tp)]
-    for step in (1, -1):
-        for c in range(2):
-            partners.append((2 * ((chip + chips + step) % chips) + c, tp))
     for dx in range(1, tps):
         for c in range(2):
             partners.append((2 * chip + c, (tp + dx) % tps))
+    has_left, has_right = chip > 0, chip < chips - 1
+    has_far_left, has_far_right = chip > 1, chip < chips - 2
+    after, before = jnp.minimum(chip + 1, chips - 1), jnp.maximum(chip - 1, 0)
     for partner in partners:
         pl.semaphore_signal(barrier, inc=1, device_id=partner, device_id_type=MESH)
+    for has, neighbour in ((has_left, before), (has_right, after)):
+        @pl.when(has)
+        def _():
+            for c in range(2):
+                pl.semaphore_signal(barrier, inc=1, device_id=(2 * neighbour + c, tp), device_id_type=MESH)
+
+    angles = (sp * TOK + iota((TOK, HEAD_DIM), 0)).astype(F32) * frequency[...]
+    cos[...] = jnp.cos(angles)
+    sine = jnp.sin(angles)
+    sin[...] = jnp.where(iota((TOK, HEAD_DIM), 1) < HEAD_DIM // 2, -sine, sine)
 
     def row_of(at, size):
         return pl.ds(pl.multiple_of(at, 128), size)
@@ -101,23 +111,32 @@
         return pltpu.make_async_remote_copy(src_ref=src, dst_ref=dst, send_sem=send, recv_sem=recv,
                                             device_id=device, device_id_type=MESH)
 
-    after, before = (chip + 1) % chips, (chip + chips - 1) % chips
-
-    def near_sends(s):
+
+    def near_sends(s, way):
         copies = []
+        base, to = ((BLK, after), (WIDE + CHIP, before))[way]
         for piece, (src, at, size) in enumerate(((128 * core, 512 * core, BLK), (BLK * (1 - core), BLK + 128 * core, 128))):
             for h in range(2):
-                for way, (base, to) in enumerate(((BLK, after), (WIDE + CHIP, before))):
-                    copies.append(remote(kvown.at[s, h, row_of(src, size)], kvbuf.at[s, row_of(base + at, size)],
-                                         kv_send.at[s, 4 * piece + 2 * h + way],
-                                         kv_recv.at[s, 4 * way + 2 * piece + core], (2 * to + h, tp)))
+                copies.append(remote(kvown.at[s, h, row_of(src, size)], kvbuf.at[s, row_of(base + at, size)],
+                                     kv_send.at[s, 4 * piece + 2 * h + way],
+                                     kv_recv.at[s, 4 * way + 2 * piece + core], (2 * to + h, tp)))
         return copies
 
-    def far_sends(s):
-        return [remote(kvbuf.at[s, pl.ds(WIDE - BLK, BLK)], kvbuf.at[s, pl.ds(0, BLK)],
-                       kv_send.at[s, 8], kv_recv.at[s, 8], (2 * after + core, tp)),
-                remote(kvbuf.at[s, pl.ds(WIDE + CHIP, BLK)], kvbuf.at[s, pl.ds(ROWS - BLK, BLK)],
-                       kv_send.at[s, 9], kv_recv.at[s, 9], (2 * before + core, tp))]
+    def far_send(s, way):
+        src, dst, to = ((WIDE - BLK, 0, after), (WIDE + CHIP, ROWS - BLK, before))[way]
+        return remote(kvbuf.at[s, pl.ds(src, BLK)], kvbuf.at[s, pl.ds(dst, BLK)],
+                      kv_send.at[s, 8 + way], kv_recv.at[s, 8 + way], (2 * to + core, tp))
+
+    sends_to = (has_right, has_left)
+    hears_from = (has_left, has_right)
+    hears_far = (has_far_left, has_far_right)
+
+    def start_near(s):
+        for way in range(2):
+            @pl.when(sends_to[way])
+            def _():
+                for copy in near_sends(s, way):
+                    copy.start()
 
     def own_sends(s):
         return [remote(kvown.at[s, 1 - core], kvbuf.at[s, row_of(WIDE + TOK * core, TOK)],
@@ -191,9 +210,8 @@
 
         @pl.when(s == 0)
         def _():
-            pl.semaphore_wait(barrier, len(partners))
-            for copy in near_sends(0):
-                copy.start()
+            pl.semaphore_wait(barrier, len(partners) + 2 * (jnp.where(has_left, 1, 0) + jnp.where(has_right, 1, 0)))
+            start_near(0)
         own_sends(s)[0].start()
         local_copies(s)[0].start()
 
@@ -343,29 +361,44 @@
             logs[s, 0:1, lanes] = upper[piece:piece + 1]
             logs[s, 1:2, lanes] = lower[piece:piece + 1]
 
+    for has, at, size in ((has_left, BLK, CHIP), (has_far_left, 0, BLK),
+                          (has_right, WIDE + CHIP, CHIP), (has_far_right, ROWS - BLK, BLK)):
+        @pl.when(jnp.logical_not(has))
+        def _():
+            def clear(s, _):
+                kvbuf[s, pl.ds(at, size), :] = jnp.zeros((size, 2 * HEAD_DIM), BF16)
+                return 0
+            lax.fori_loop(0, seqs, clear, 0)
+
     def stage(s, _):
-        near_arrival(s, 0, 0, 1).wait_recv()
-        near_arrival(s, 1, 0, 0).wait_recv()
-        for copy in far_sends(s):
-            copy.start()
+        for way in range(2):
+            @pl.when(hears_from[way])
+            def _():
+                near_arrival(s, way, 0, 1 - way).wait_recv()
+
+            @pl.when(jnp.logical_and(hears_from[way], sends_to[way]))
+            def _():
+                far_send(s, way).start()
 
         @pl.when(s + 1 < seqs)
         def _():
-            for copy in near_sends(s + 1):
-                copy.start()
+            start_near(s + 1)
 
         for copy in local_copies(s):
             copy.wait()
         for copy in own_arrivals(s):
             copy.wait_recv()
-        near_arrival(s, 0, 0, 0).wait_recv()
-        near_arrival(s, 1, 0, 1).wait_recv()
         for way in range(2):
-            for c in range(2):
-                near_arrival(s, way, 1, c).wait_recv()
+            @pl.when(hears_from[way])
+            def _():
+                near_arrival(s, way, 0, way).wait_recv()
+                for c in range(2):
+                    near_arrival(s, way, 1, c).wait_recv()
         near(s)
-        for copy in far_sends(s):
-            copy.wait_recv()
+        for way in range(2):
+            @pl.when(hears_far[way])
+            def _():
+                far_send(s, way).wait_recv()
         far(s)
 
         @pl.when(s > 0)
@@ -377,8 +410,17 @@
     finish(seqs - 1)
 
     def drain(s, _):
-        for copy in near_sends(s) + far_sends(s) + own_sends(s):
+        for copy in own_sends(s):
             copy.wait_send()
+        for way in range(2):
+            @pl.when(sends_to[way])
+            def _():
+                for copy in near_sends(s, way):
+                    copy.wait_send()
+
+            @pl.when(jnp.logical_and(hears_from[way], sends_to[way]))
+            def _():
+                far_send(s, way).wait_send()
         for copy in x_sends(s):
             copy.wait_send()
         pltpu.make_async_copy(out_v.at[s], out.at[s], out_sem.at[s]).wait()
@@ -389,24 +431,22 @@
 def shards(chips, tps, tokens, query_weight, key_weight, value_weight, out_gain, out_weight):
     seqs, length, model_dim = tokens.shape
     channels, out_cols = out_weight.shape
-    positions = lax.axis_index("sp") * length + jnp.arange(length, dtype=jnp.int32)
     half_dim = HEAD_DIM // 2
     frequency = ROPE_BASE ** (-jnp.arange(half_dim, dtype=F32) / half_dim)
-    angles = positions.astype(F32)[:, None] * frequency[None, :]
-    cosine, sine = jnp.cos(angles), jnp.sin(angles)
-    cosine = jnp.concatenate([cosine, cosine], axis=1)
-    sine = jnp.concatenate([-sine, sine], axis=1)
+    frequency = jnp.concatenate([frequency, frequency]).reshape(1, HEAD_DIM)
     any_spec = pl.BlockSpec(memory_space=pl.ANY)
     vmem = pl.BlockSpec(memory_space=pltpu.VMEM)
     dma = pltpu.SemaphoreType.DMA
     grid4 = (OWN, 4, 4, 16, HEAD_DIM)
     return pl.pallas_call(
         functools.partial(kernel, chips, tps, seqs),
-        out_shape=(jax.ShapeDtypeStruct((seqs, length, out_cols), BF16),
+        out_shape=(pltpu.VMEM((seqs, length, out_cols), BF16),
                    jax.ShapeDtypeStruct((seqs, 2, length), F32)),
-        in_specs=[any_spec, any_spec, any_spec, any_spec, vmem, any_spec, vmem, vmem],
+        in_specs=[any_spec, any_spec, any_spec, any_spec, vmem, any_spec, vmem],
         out_specs=(any_spec, vmem),
         scratch_shapes=[
+            pltpu.VMEM((TOK, HEAD_DIM), F32),
+            pltpu.VMEM((TOK, HEAD_DIM), F32),
             pltpu.VMEM((seqs, TOK, model_dim), BF16),
             pltpu.VMEM((model_dim, 256), BF16),
             pltpu.VMEM((model_dim, 256), BF16),
@@ -444,9 +484,9 @@
             dma((seqs,)),
         ],
         compiler_params=pltpu.CompilerParams(
-            collective_id=0, has_side_effects=True, vmem_limit_bytes=60 * 1024 * 1024
+            collective_id=0, has_side_effects=True, vmem_limit_bytes=62 * 1024 * 1024
         ),
-    )(tokens, query_weight, key_weight, value_weight, out_gain.reshape(1, channels), out_weight, cosine, sine)
+    )(tokens, query_weight, key_weight, value_weight, out_gain.reshape(1, channels), out_weight, frequency)
 
 
 def solution(mesh):

time: 84.4 us -> 75.5 us (0.89)
  the two profiles are of different devices: /device:TPU:1 before, /device:TPU:193 now
where the time goes in v2:
time: 75.5 us; the launch traced here: 75.4 us
  Pallas kernels  72.4 us (96%)
  local copies, waits for them, and re-layouts  1.75 us (2%)
    pallas_call x1, Pallas kernels, shards(): pl.pallas_call(functools.partial(kernel, chips, tps, seqs), out_shape=(pl...  72.4 us
    unnamed x4, local copies, waits for them, and re-layouts  1.75 us

profile of v2, /device:TPU:193, one launch (start us, length us, event | category | flops | bytes accessed | tf_op | source)
XLA Modules:
  0.0 75.4 jit_solution(1225022556956079144)
XLA Ops:
  0.6 0.6 maximum_bitcast_fusion.frequency
  1.2 72.4 %shard_map.77 = (bf16[4,384,512]{2,1,0:T(8,128)(2,1)S(1)}, f32[4,2,384]{2,1,0:T(2,128)}) custom-call(bf16[4,384,2048]{2,1,0:T(8,128)(2,1)} %tokens.1, bf16[2048,256]{1,0:T(8,128)(2,1)} %wq.1, bf16[2048,256]{1,0:T(8,128)(2,1)} %wk.1, bf16[2048,256]{1,0:T(8,128)(2,1)} %wv.1, f32[1,1024]{1,0:T(1,128)} %bitcast.3, bf16[1024,512]{1,0:T(8,128)(2,1)} %wo.1, ...), custom_call_target="tpu_custom_call" | custom-call | tf_op jit(solution)/shard_map/pallas_call | solution.py:441
  73.7 0.0 copy-start
  73.7 1.1 %copy.10 = bf16[4,384,512]{2,1,0:T(8,128)(2,1)} copy(bf16[4,384,512]{2,1,0:T(8,128)(2,1)S(1)} %get-tuple-element.2) | data formatting | bytes 3145728
  74.8 0.0 copy-done
  74.8 0.6 copy.11
  (1 shorter events, 0.0 us)
Async XLA Ops:
  73.7 1.2 %copy-start = (f32[4,2,384]{2,1,0:T(2,128)S(1)}, f32[4,2,384]{2,1,0:T(2,128)}, u32[]{:S(2)}) copy-start(f32[4,2,384]{2,1,0:T(2,128)} %get-tuple-element.7) | copy-start | bytes 36868

commit v3 on v2

--- a/solution.py
+++ b/solution.py
@@ -68,7 +68,7 @@
 
 def kernel(chips, tps, seqs, tokens, wq, wk, wv, gain, wo, frequency, out, logs,
            cos, sin, tok_v, wq_v, wk_v, wv_v, wo_v, kvown, qown, kvbuf, qbuf, kvp, qp, perm,
-           bias1, bias4, bias16, acc1, peak1, sum1, mperm, lperm, mnat, lnat, lrx, mg, out_v,
+           bias1, bias4, bias_mid, bias_out, acc1, peak1, sum1, mperm, lperm, mnat, lnat, lrx, mg, out_v,
            in_sem, loc_sem, kv_send, kv_recv, x_send, x_recv, l_send, l_recv, x_loc, out_sem):
     sp, tp = lax.axis_index("sp"), lax.axis_index("tp")
     chip, core = sp // 2, sp % 2
@@ -80,7 +80,7 @@
     for s in range(1, seqs):
         loads.append(pltpu.make_async_copy(tokens.at[s], tok_v.at[s], in_sem.at[4 + s]))
     loads.append(pltpu.make_async_copy(wo, wo_v, in_sem.at[3]))
-    for load in loads:
+    for load in loads[:3]:
         load.start()
 
     barrier = pltpu.get_barrier_semaphore()
@@ -165,27 +165,36 @@
     def column_of(h):
         return pl.ds(pl.multiple_of(h * HEAD_DIM, HEAD_DIM), HEAD_DIM)
 
-    def x_sends(s):
+    def piece_of(piece, c):
+        return ((BLK * (1 - c), 128), (128 * c, BLK))[piece]
+
+    def x_sends(s, piece):
         copies = []
-        for dx in range(1, tps):
-            for c in range(2):
-                copies.append(remote(mnat.at[s, pl.ds(TOK * c, TOK)], mg.at[s, :, column_of(head)],
-                                     x_send.at[s, 2 * dx + c], x_recv.at[s, head], (2 * chip + c, (tp + dx) % tps)))
-        copies.append(remote(mnat.at[s, row_of(TOK * (1 - core), TOK)], mg.at[s, :, column_of(head)],
-                             x_send.at[s, 0], x_recv.at[s, head], (2 * chip + 1 - core, tp)))
-        copies.append(remote(lnat.at[s, 1 - core], lrx.at[s], l_send.at[s], l_recv.at[s], (2 * chip + 1 - core, tp)))
+        for dx in [tps // 2] + [d for d in range(1, tps) if d != tps // 2]:
+            for c in range(2) if tps > 1 else ():
+                at, size = piece_of(piece, c)
+                copies.append(remote(mnat.at[s, pl.ds(TOK * c + at, size)], mg.at[s, pl.ds(at, size), column_of(head)],
+                                     x_send.at[s, 8 * piece + 2 * dx + c], x_recv.at[s, 8 * piece + head],
+                                     (2 * chip + c, (tp + dx) % tps)))
+        at, size = piece_of(piece, 1 - core)
+        copies.append(remote(mnat.at[s, row_of(TOK * (1 - core) + at, size)], mg.at[s, row_of(at, size), column_of(head)],
+                             x_send.at[s, 8 * piece], x_recv.at[s, 8 * piece + head], (2 * chip + 1 - core, tp)))
         return copies
+
+    def log_send(s):
+        return remote(lnat.at[s, 1 - core], lrx.at[s], l_send.at[s], l_recv.at[s], (2 * chip + 1 - core, tp))
 
     def x_local(s):
         return pltpu.make_async_copy(mnat.at[s, row_of(TOK * core, TOK)], mg.at[s, :, column_of(head)], x_loc.at[s])
 
     def x_arrivals(s):
         waits = []
-        for o in range(1, 2 * tps):
-            other = (head + o) % (2 * tps)
-            waits.append(remote(mnat.at[s, pl.ds(0, TOK)], mg.at[s, :, column_of(other)], x_send.at[s, 0],
-                                x_recv.at[s, other], (2 * chip + 1 - core, tp)))
-        waits.append(remote(lnat.at[s, 0], lrx.at[s], l_send.at[s], l_recv.at[s], (2 * chip + 1 - core, tp)))
+        for piece in range(2):
+            at, size = piece_of(piece, core)
+            for o in range(1, 2 * tps):
+                other = (head + o) % (2 * tps)
+                waits.append(remote(mnat.at[s, pl.ds(0, size)], mg.at[s, row_of(at, size), column_of(other)],
+                                    x_send.at[s, 0], x_recv.at[s, 8 * piece + other], (2 * chip + 1 - core, tp)))
         return waits
 
     def turned(x):
@@ -197,13 +206,13 @@
         @pl.when(s == 0)
         def _():
             loads[0].wait()
+            loads[2].wait()
+            for load in loads[3:]:
+                load.start()
         keys = dot(tok_v[s], wk_v[...])
         for h in range(2):
             kvown[s, h, :, :HEAD_DIM] = turned(keys[:, h * HEAD_DIM:(h + 1) * HEAD_DIM])
 
-        @pl.when(s == 0)
-        def _():
-            loads[2].wait()
         values = dot(tok_v[s], wv_v[...])
         for h in range(2):
             kvown[s, h, :, HEAD_DIM:] = values[:, h * HEAD_DIM:(h + 1) * HEAD_DIM].astype(BF16)
@@ -243,12 +252,15 @@
         at = first + (b + col // 64 - 1) * BLK
         good = (gap >= -REACH) & (gap <= REACH) & (at >= 0) & (at < limit)
         bias4[b] = jnp.where(good, 0.0, MASK_FILL)
-    row, col = iota((16 * OWN, 16 * NBLK), 0), iota((16 * OWN, 16 * NBLK), 1)
-    gap = row - (col - 16 * HALO)
-    at = first + (col // 16 - HALO) * BLK
-    good = (gap >= -REACH) & (gap <= REACH) & (at >= 0) & (at < limit)
-    bias16[...] = jnp.where(good, 0.0, MASK_FILL)
-
+    for ref, q_blocks, k_blocks in ((bias_mid, (1,), range(1, NBLK - 1)), (bias_out, (0, 2), range(NBLK))):
+        dims = (16 * len(q_blocks), 16 * len(k_blocks))
+        row, col = iota(dims, 0), iota(dims, 1)
+        q_at = row % 16 + 16 * (q_blocks[0] + 2 * (row // 16))
+        block = col // 16 + k_blocks[0] - HALO
+        gap = q_at - (col % 16 + 16 * block)
+        at = first + block * BLK
+        good = (gap >= -REACH) & (gap <= REACH) & (at >= 0) & (at < limit)
+        ref[...] = jnp.where(good, 0.0, MASK_FILL)
 
     def put_in_order(s, blocks):
         for b in blocks:
@@ -298,40 +310,49 @@
                         sum1[b, a, r] = jnp.broadcast_to(total, (16, HEAD_DIM))
             return scores, finish
 
-        for b in range(OWN):
+        pipelined([narrow(1, 0), narrow(1, 1), middle(1)] + [wide(r, (1,), range(1, NBLK - 1), bias_mid) for r in range(4)])
+        in_order(s, 1)
+        for copy in x_sends(s, 0):
+            copy.start()
+        for b in (0, 2):
             jobs += [narrow(b, 0), narrow(b, 1), middle(b)]
         pipelined(jobs)
 
+    def wide(r, q_blocks, k_blocks, bias):
+        keys_in = slice(k_blocks[0], k_blocks[-1] + 1)
+
+        def scores():
+            every = []
+            for a in range(4):
+                keys = kvp[keys_in, a, r, :, :HEAD_DIM].reshape(16 * len(k_blocks), HEAD_DIM)
+                queries = jnp.concatenate([qp[b, a, r] for b in q_blocks], axis=0)
+                every.append(dot_nt(queries, keys) + bias[...])
+            return every
+
+        def finish(every):
+            soft = [softened(scores) for scores in every]
+            accs = []
+            for a in range(4):
+                values = kvp[keys_in, a, r, :, HEAD_DIM:].reshape(16 * len(k_blocks), HEAD_DIM)
+                accs.append(dot(soft[a][0], values))
+            for a in range(4):
+                for i, b in enumerate(q_blocks):
+                    one = (acc1[b, a, r], peak1[b, a, r], sum1[b, a, r])
+                    two = tuple(x[i * 16:(i + 1) * 16] for x in (accs[a],) + soft[a][1:])
+                    merged, peak, total = joined((one, two))
+                    mperm[b, a, r] = (merged / total).astype(BF16)
+                    lperm[b, a, r] = peak * SCALE + jnp.log(total)
+        return scores, finish
+
+    def in_order(s, b):
+        mnat[s, pl.ds(b * BLK, BLK), :] = dot(perm[...], mperm[b].reshape(BLK, HEAD_DIM)).astype(BF16)
+
     def far(s):
         put_in_order(s, (0, NBLK - 1))
-
-        def wide(r):
-            def scores():
-                every = []
-                for a in range(4):
-                    keys = kvp[:, a, r, :, :HEAD_DIM].reshape(16 * NBLK, HEAD_DIM)
-                    every.append(dot_nt(qp[:, a, r].reshape(16 * OWN, HEAD_DIM), keys) + bias16[...])
-                return every
-
-            def finish(every):
-                soft = [softened(scores) for scores in every]
-                accs = []
-                for a in range(4):
-                    values = kvp[:, a, r, :, HEAD_DIM:].reshape(16 * NBLK, HEAD_DIM)
-                    accs.append(dot(soft[a][0], values))
-                for a in range(4):
-                    for b in range(OWN):
-                        one = (acc1[b, a, r], peak1[b, a, r], sum1[b, a, r])
-                        two = tuple(x[b * 16:(b + 1) * 16] for x in (accs[a],) + soft[a][1:])
-                        merged, peak, total = joined((one, two))
-                        mperm[b, a, r] = (merged / total).astype(BF16)
-                        lperm[b, a, r] = peak * SCALE + jnp.log(total)
-            return scores, finish
-
-        pipelined([wide(r) for r in range(4)])
-        for b in range(OWN):
-            mnat[s, pl.ds(b * BLK, BLK), :] = dot(perm[...], mperm[b].reshape(BLK, HEAD_DIM)).astype(BF16)
-        for copy in x_sends(s)[:-1]:
+        pipelined([wide(r, (0, 2), range(NBLK), bias_out) for r in range(4)])
+        for b in (0, 2):
+            in_order(s, b)
+        for copy in x_sends(s, 1):
             copy.start()
         x_local(s).start()
         for b in range(OWN):
@@ -341,12 +362,13 @@
                 line = jnp.sum(jnp.where(hit > 0.5, column, 0.0), axis=0, keepdims=True)
                 piece = 2 * b + half
                 lnat[s, piece // 3, piece % 3:piece % 3 + 1, :] = line
-        x_sends(s)[-1].start()
+        log_send(s).start()
 
     def finish(s):
         x_local(s).wait()
         for copy in x_arrivals(s):
             copy.wait_recv()
+        log_send(s).wait_recv()
         lifted = mg[s].astype(F32)
         square = jnp.mean(lifted * lifted, axis=-1, keepdims=True)
         scaled = (lifted * gain[...]).astype(BF16)
@@ -421,8 +443,9 @@
             @pl.when(jnp.logical_and(hears_from[way], sends_to[way]))
             def _():
                 far_send(s, way).wait_send()
-        for copy in x_sends(s):
+        for copy in x_sends(s, 0) + x_sends(s, 1):
             copy.wait_send()
+        log_send(s).wait_send()
         pltpu.make_async_copy(out_v.at[s], out.at[s], out_sem.at[s]).wait()
         return 0
     lax.fori_loop(0, seqs, drain, 0)
@@ -432,8 +455,8 @@
     seqs, length, model_dim = tokens.shape
     channels, out_cols = out_weight.shape
     half_dim = HEAD_DIM // 2
-    frequency = ROPE_BASE ** (-jnp.arange(half_dim, dtype=F32) / half_dim)
-    frequency = jnp.concatenate([frequency, frequency]).reshape(1, HEAD_DIM)
+    frequency = ROPE_BASE ** (-(jnp.arange(HEAD_DIM) % half_dim).astype(F32) / half_dim)
+    frequency = frequency.reshape(1, HEAD_DIM)
     any_spec = pl.BlockSpec(memory_space=pl.ANY)
     vmem = pl.BlockSpec(memory_space=pltpu.VMEM)
     dma = pltpu.SemaphoreType.DMA
@@ -461,7 +484,8 @@
             pltpu.VMEM((BLK, BLK), BF16),
             pltpu.VMEM((OWN, BLK, BLK + 2 * REACH), F32),
             pltpu.VMEM((OWN, 64, 192), F32),
-            pltpu.VMEM((16 * OWN, 16 * NBLK), F32),
+            pltpu.VMEM((16, 16 * (NBLK - 2)), F32),
+            pltpu.VMEM((32, 16 * NBLK), F32),
             pltpu.VMEM(grid4, F32),
             pltpu.VMEM(grid4, F32),
             pltpu.VMEM(grid4, F32),
@@ -476,8 +500,8 @@
             dma((seqs, 2)),
             dma((seqs, 12)),
             dma((seqs, 12)),
-            dma((seqs, 8)),
-            dma((seqs, 8)),
+            dma((seqs, 16)),
+            dma((seqs, 16)),
             dma((seqs,)),
             dma((seqs,)),
             dma((seqs,)),

time: 75.5 us -> 73.2 us (0.970)
  Pallas kernels: 72.4 us -> 70.1 us
    pallas_call x1, Pallas kernels: 72.4 us -> 70.1 us  [shards(): pl.pallas_call(functools.partial(kernel, chips, tps, seqs), out_shape=(pl...]
where the time goes in v3:
time: 73.2 us; the launch traced here: 73 us
  Pallas kernels  70.1 us (96%)
  local copies, waits for them, and re-layouts  1.75 us (2%)
    pallas_call x1, Pallas kernels, shards(): pl.pallas_call(functools.partial(kernel, chips, tps, seqs), out_shape=(pl...  70.1 us
    unnamed x4, local copies, waits for them, and re-layouts  1.75 us

profile of v3, /device:TPU:193, one launch (start us, length us, event | category | flops | bytes accessed | tf_op | source)
XLA Modules:
  0.0 73.0 jit_solution(172855719233531331)
XLA Ops:
  0.6 0.5 fusion.3.frequency
  1.2 70.1 %shard_map.77 = (bf16[4,384,512]{2,1,0:T(8,128)(2,1)S(1)}, f32[4,2,384]{2,1,0:T(2,128)}) custom-call(bf16[4,384,2048]{2,1,0:T(8,128)(2,1)} %tokens.1, bf16[2048,256]{1,0:T(8,128)(2,1)} %wq.1, bf16[2048,256]{1,0:T(8,128)(2,1)} %wk.1, bf16[2048,256]{1,0:T(8,128)(2,1)} %wv.1, f32[1,1024]{1,0:T(1,128)} %bitcast.1, bf16[1024,512]{1,0:T(8,128)(2,1)} %wo.1, ...), custom_call_target="tpu_custom_call" | custom-call | tf_op jit(solution)/shard_map/pallas_call | solution.py:464
  71.3 0.0 copy-start
  71.3 1.1 %copy.10 = bf16[4,384,512]{2,1,0:T(8,128)(2,1)} copy(bf16[4,384,512]{2,1,0:T(8,128)(2,1)S(1)} %get-tuple-element.2) | data formatting | bytes 3145728
  72.4 0.0 copy-done
  72.4 0.6 copy.11
Async XLA Ops:
  71.3 1.2 %copy-start = (f32[4,2,384]{2,1,0:T(2,128)S(1)}, f32[4,2,384]{2,1,0:T(2,128)}, u32[]{:S(2)}) copy-start(f32[4,2,384]{2,1,0:T(2,128)} %get-tuple-element.7) | copy-start | bytes 36868

commit v4 on v3

--- a/solution.py
+++ b/solution.py
@@ -1,4 +1,5 @@
 import functools
+import math
 
 import jax
 import jax.numpy as jnp
@@ -66,21 +67,26 @@
     return lax.broadcasted_iota(jnp.int32, shape, dim)
 
 
-def kernel(chips, tps, seqs, tokens, wq, wk, wv, gain, wo, frequency, out, logs,
-           cos, sin, tok_v, wq_v, wk_v, wv_v, wo_v, kvown, qown, kvbuf, qbuf, kvp, qp, perm,
+def kernel(chips, tps, seqs, tokens, wq, wk, wv, gain_in, wo, out, logs,
+           cos, sin, gain, tok_v, wq_v, wkv_v, wo_v, kvown, qown, kvbuf, qbuf, kvp, qp, perm,
            bias1, bias4, bias_mid, bias_out, acc1, peak1, sum1, mperm, lperm, mnat, lnat, lrx, mg, out_v,
            in_sem, loc_sem, kv_send, kv_recv, x_send, x_recv, l_send, l_recv, x_loc, out_sem):
     sp, tp = lax.axis_index("sp"), lax.axis_index("tp")
     chip, core = sp // 2, sp % 2
 
-    loads = [pltpu.make_async_copy(wk, wk_v, in_sem.at[0]),
-             pltpu.make_async_copy(tokens.at[0], tok_v.at[0], in_sem.at[4]),
-             pltpu.make_async_copy(wv, wv_v, in_sem.at[1]),
-             pltpu.make_async_copy(wq, wq_v, in_sem.at[2])]
-    for s in range(1, seqs):
-        loads.append(pltpu.make_async_copy(tokens.at[s], tok_v.at[s], in_sem.at[4 + s]))
-    loads.append(pltpu.make_async_copy(wo, wo_v, in_sem.at[3]))
-    for load in loads[:3]:
+    def token_load(s):
+        return pltpu.make_async_copy(tokens.at[s], tok_v.at[s], in_sem.at[s])
+
+    def pair_loads(h):
+        lanes = pl.ds(h * HEAD_DIM, HEAD_DIM)
+        return [pltpu.make_async_copy(w.at[:, lanes], wkv_v.at[h, :, pl.ds(i * HEAD_DIM, HEAD_DIM)],
+                                      in_sem.at[seqs + 2 * h + i]) for i, w in enumerate((wk, wv))]
+
+    query_load = pltpu.make_async_copy(wq, wq_v, in_sem.at[seqs + 4])
+    last_loads = [pltpu.make_async_copy(wo, wo_v, in_sem.at[seqs + 5]),
+                  pltpu.make_async_copy(gain_in, gain, in_sem.at[seqs + 6])]
+    token_load(0).start()
+    for load in pair_loads(0) + pair_loads(1):
         load.start()
 
     barrier = pltpu.get_barrier_semaphore()
@@ -99,7 +105,9 @@
             for c in range(2):
                 pl.semaphore_signal(barrier, inc=1, device_id=(2 * neighbour + c, tp), device_id_type=MESH)
 
-    angles = (sp * TOK + iota((TOK, HEAD_DIM), 0)).astype(F32) * frequency[...]
+    pair = iota((1, HEAD_DIM), 1) % (HEAD_DIM // 2)
+    frequency = jnp.exp2(pair.astype(F32) * (-math.log2(ROPE_BASE) / (HEAD_DIM // 2)))
+    angles = (sp * TOK + iota((TOK, HEAD_DIM), 0)).astype(F32) * frequency
     cos[...] = jnp.cos(angles)
     sine = jnp.sin(angles)
     sin[...] = jnp.where(iota((TOK, HEAD_DIM), 1) < HEAD_DIM // 2, -sine, sine)
@@ -131,11 +139,11 @@
     hears_from = (has_left, has_right)
     hears_far = (has_far_left, has_far_right)
 
-    def start_near(s):
+    def start_near(s, which=slice(0, 4)):
         for way in range(2):
             @pl.when(sends_to[way])
             def _():
-                for copy in near_sends(s, way):
+                for copy in near_sends(s, way)[which]:
                     copy.start()
 
     def own_sends(s):
@@ -201,32 +209,36 @@
         return (x * cos[...] + pltpu.roll(x, HEAD_DIM // 2, 1) * sin[...]).astype(BF16)
 
     def project(s, _):
-        pltpu.make_async_copy(tokens.at[s], tok_v.at[s], in_sem.at[4 + s]).wait()
+        token_load(s).wait()
+        for h in range(2):
+            @pl.when(s == 0)
+            def _():
+                for load in pair_loads(h):
+                    load.wait()
+                if h == 1:
+                    for t in range(1, seqs):
+                        token_load(t).start()
+                    for load in last_loads:
+                        load.start()
+                else:
+                    query_load.start()
+            both = dot(tok_v[s], wkv_v[h])
+            kvown[s, h, :, :HEAD_DIM] = turned(both[:, :HEAD_DIM])
+            kvown[s, h, :, HEAD_DIM:] = both[:, HEAD_DIM:].astype(BF16)
+
+            @pl.when(s == 0)
+            def _():
+                if h == 0:
+                    pl.semaphore_wait(barrier, len(partners) + 2 * (jnp.where(has_left, 1, 0) + jnp.where(has_right, 1, 0)))
+                    start_near(0, slice(0, 1))
+                else:
+                    start_near(0, slice(1, 4))
+        own_sends(s)[0].start()
+        local_copies(s)[0].start()
 
         @pl.when(s == 0)
         def _():
-            loads[0].wait()
-            loads[2].wait()
-            for load in loads[3:]:
-                load.start()
-        keys = dot(tok_v[s], wk_v[...])
-        for h in range(2):
-            kvown[s, h, :, :HEAD_DIM] = turned(keys[:, h * HEAD_DIM:(h + 1) * HEAD_DIM])
-
-        values = dot(tok_v[s], wv_v[...])
-        for h in range(2):
-            kvown[s, h, :, HEAD_DIM:] = values[:, h * HEAD_DIM:(h + 1) * HEAD_DIM].astype(BF16)
-
-        @pl.when(s == 0)
-        def _():
-            pl.semaphore_wait(barrier, len(partners) + 2 * (jnp.where(has_left, 1, 0) + jnp.where(has_right, 1, 0)))
-            start_near(0)
-        own_sends(s)[0].start()
-        local_copies(s)[0].start()
-
-        @pl.when(s == 0)
-        def _():
-            loads[3].wait()
+            query_load.wait()
         queries = dot(tok_v[s], wq_v[...])
         for h in range(2):
             qown[s, h] = turned(queries[:, h * HEAD_DIM:(h + 1) * HEAD_DIM])
@@ -235,7 +247,8 @@
         return 0
 
     lax.fori_loop(0, seqs, project, 0)
-    loads[-1].wait()
+    for load in last_loads:
+        load.wait()
 
     row, col = iota((BLK, BLK), 0), iota((BLK, BLK), 1)
     perm[...] = jnp.where(col == (row % 16) * 16 + row // 16, 1.0, 0.0).astype(BF16)
@@ -454,9 +467,6 @@
 def shards(chips, tps, tokens, query_weight, key_weight, value_weight, out_gain, out_weight):
     seqs, length, model_dim = tokens.shape
     channels, out_cols = out_weight.shape
-    half_dim = HEAD_DIM // 2
-    frequency = ROPE_BASE ** (-(jnp.arange(HEAD_DIM) % half_dim).astype(F32) / half_dim)
-    frequency = frequency.reshape(1, HEAD_DIM)
     any_spec = pl.BlockSpec(memory_space=pl.ANY)
     vmem = pl.BlockSpec(memory_space=pltpu.VMEM)
     dma = pltpu.SemaphoreType.DMA
@@ -465,15 +475,15 @@
         functools.partial(kernel, chips, tps, seqs),
         out_shape=(pltpu.VMEM((seqs, length, out_cols), BF16),
                    jax.ShapeDtypeStruct((seqs, 2, length), F32)),
-        in_specs=[any_spec, any_spec, any_spec, any_spec, vmem, any_spec, vmem],
+        in_specs=[any_spec] * 6,
         out_specs=(any_spec, vmem),
         scratch_shapes=[
             pltpu.VMEM((TOK, HEAD_DIM), F32),
             pltpu.VMEM((TOK, HEAD_DIM), F32),
+            pltpu.VMEM((1, channels), F32),
             pltpu.VMEM((seqs, TOK, model_dim), BF16),
             pltpu.VMEM((model_dim, 256), BF16),
-            pltpu.VMEM((model_dim, 256), BF16),
-            pltpu.VMEM((model_dim, 256), BF16),
+            pltpu.VMEM((2, model_dim, 256), BF16),
             pltpu.VMEM((channels, out_cols), BF16),
             pltpu.VMEM((seqs, 2, TOK, 256), BF16),
             pltpu.VMEM((seqs, 2, TOK, 128), BF16),
@@ -496,7 +506,7 @@
             pltpu.VMEM((seqs, 3, 128), F32),
             pltpu.VMEM((seqs, TOK, channels), BF16),
             pltpu.VMEM((seqs, TOK, out_cols), BF16),
-            dma((4 + seqs,)),
+            dma((7 + seqs,)),
             dma((seqs, 2)),
             dma((seqs, 12)),
             dma((seqs, 12)),
@@ -510,7 +520,7 @@
         compiler_params=pltpu.CompilerParams(
             collective_id=0, has_side_effects=True, vmem_limit_bytes=62 * 1024 * 1024
         ),
-    )(tokens, query_weight, key_weight, value_weight, out_gain.reshape(1, channels), out_weight, frequency)
+    )(tokens, query_weight, key_weight, value_weight, out_gain.reshape(1, channels), out_weight)
 
 
 def solution(mesh):

time: 73.2 us -> 73 us (level)
  no operation moved by 1% of the time
where the time goes in v4:
time: 73 us; the launch traced here: 72.9 us
  Pallas kernels  70.5 us (97%)
  local copies, waits for them, and re-layouts  1.75 us (2%)
    pallas_call x1, Pallas kernels, shards(): pl.pallas_call(functools.partial(kernel, chips, tps, seqs), out_shape=(pl...  70.5 us
    unnamed x4, local copies, waits for them, and re-layouts  1.75 us

profile of v4, /device:TPU:193, one launch (start us, length us, event | category | flops | bytes accessed | tf_op | source)
XLA Modules:
  0.0 72.9 jit_solution(11187311127482007152)
XLA Ops:
  0.6 70.5 %shard_map.77 = (bf16[4,384,512]{2,1,0:T(8,128)(2,1)S(1)}, f32[4,2,384]{2,1,0:T(2,128)}) custom-call(bf16[4,384,2048]{2,1,0:T(8,128)(2,1)} %tokens.1, bf16[2048,256]{1,0:T(8,128)(2,1)} %wq.1, bf16[2048,256]{1,0:T(8,128)(2,1)} %wk.1, bf16[2048,256]{1,0:T(8,128)(2,1)} %wv.1, f32[1,1024]{1,0:T(1,128)} %bitcast.1, bf16[1024,512]{1,0:T(8,128)(2,1)} %wo.1), custom_call_target="tpu_custom_call" | custom-call | tf_op jit(solution)/shard_map/pallas_call | solution.py:474
  71.1 0.0 copy-start
  71.1 1.1 %copy.10 = bf16[4,384,512]{2,1,0:T(8,128)(2,1)} copy(bf16[4,384,512]{2,1,0:T(8,128)(2,1)S(1)} %get-tuple-element.2) | data formatting | bytes 3145728
  72.3 0.0 copy-done
  72.3 0.6 copy.11
Async XLA Ops:
  71.1 1.2 %copy-start = (f32[4,2,384]{2,1,0:T(2,128)S(1)}, f32[4,2,384]{2,1,0:T(2,128)}, u32[]{:S(2)}) copy-start(f32[4,2,384]{2,1,0:T(2,128)} %get-tuple-element.7) | copy-start | bytes 36868

commit v5 on v4

--- a/solution.py
+++ b/solution.py
@@ -406,6 +406,10 @@
             lax.fori_loop(0, seqs, clear, 0)
 
     def stage(s, _):
+        @pl.when(s + 1 < seqs)
+        def _():
+            start_near(s + 1, slice(0, 1))
+
         for way in range(2):
             @pl.when(hears_from[way])
             def _():
@@ -417,7 +421,7 @@
 
         @pl.when(s + 1 < seqs)
         def _():
-            start_near(s + 1)
+            start_near(s + 1, slice(1, 4))
 
         for copy in local_copies(s):
             copy.wait()

time: 73 us -> 73.6 us (level)
  no operation moved by 1% of the time
where the time goes in v5:
time: 73.6 us; the launch traced here: 73 us
  Pallas kernels  70.6 us (96%)
  local copies, waits for them, and re-layouts  1.75 us (2%)
    pallas_call x1, Pallas kernels, shards(): pl.pallas_call(functools.partial(kernel, chips, tps, seqs), out_shape=(pl...  70.6 us
    unnamed x4, local copies, waits for them, and re-layouts  1.75 us

profile of v5, /device:TPU:193, one launch (start us, length us, event | category | flops | bytes accessed | tf_op | source)
XLA Modules:
  0.0 73.0 jit_solution(3525324053066451458)
XLA Ops:
  0.6 70.6 %shard_map.77 = (bf16[4,384,512]{2,1,0:T(8,128)(2,1)S(1)}, f32[4,2,384]{2,1,0:T(2,128)}) custom-call(bf16[4,384,2048]{2,1,0:T(8,128)(2,1)} %tokens.1, bf16[2048,256]{1,0:T(8,128)(2,1)} %wq.1, bf16[2048,256]{1,0:T(8,128)(2,1)} %wk.1, bf16[2048,256]{1,0:T(8,128)(2,1)} %wv.1, f32[1,1024]{1,0:T(1,128)} %bitcast.1, bf16[1024,512]{1,0:T(8,128)(2,1)} %wo.1), custom_call_target="tpu_custom_call" | custom-call | tf_op jit(solution)/shard_map/pallas_call | solution.py:478
  71.3 0.0 copy-start
  71.3 1.1 %copy.10 = bf16[4,384,512]{2,1,0:T(8,128)(2,1)} copy(bf16[4,384,512]{2,1,0:T(8,128)(2,1)S(1)} %get-tuple-element.2) | data formatting | bytes 3145728
  72.4 0.0 copy-done
  72.4 0.6 copy.11
Async XLA Ops:
  71.3 1.2 %copy-start = (f32[4,2,384]{2,1,0:T(2,128)S(1)}, f32[4,2,384]{2,1,0:T(2,128)}, u32[]{:S(2)}) copy-start(f32[4,2,384]{2,1,0:T(2,128)} %get-tuple-element.7) | copy-start | bytes 36868

commit v6 on v4

--- a/solution.py
+++ b/solution.py
@@ -25,6 +25,7 @@
 OWN = CHIP // BLK
 NBLK = 2 * HALO + OWN
 ROWS = NBLK * BLK
+HAND_OVER = 1024 * 1024
 MESH = pl.DeviceIdType.MESH
 F32 = jnp.float32
 BF16 = jnp.bfloat16
@@ -69,8 +70,8 @@
 
 def kernel(chips, tps, seqs, tokens, wq, wk, wv, gain_in, wo, out, logs,
            cos, sin, gain, tok_v, wq_v, wkv_v, wo_v, kvown, qown, kvbuf, qbuf, kvp, qp, perm,
-           bias1, bias4, bias_mid, bias_out, acc1, peak1, sum1, mperm, lperm, mnat, lnat, lrx, mg, out_v,
-           in_sem, loc_sem, kv_send, kv_recv, x_send, x_recv, l_send, l_recv, x_loc, out_sem):
+           bias1, bias4, bias_mid, bias_out, acc1, peak1, sum1, mperm, lperm, mnat, lnat, lrx, mg,
+           in_sem, loc_sem, kv_send, kv_recv, x_send, x_recv, l_send, l_recv, x_loc):
     sp, tp = lax.axis_index("sp"), lax.axis_index("tp")
     chip, core = sp // 2, sp % 2
 
@@ -386,8 +387,7 @@
         square = jnp.mean(lifted * lifted, axis=-1, keepdims=True)
         scaled = (lifted * gain[...]).astype(BF16)
         projected = dot(scaled, wo_v[...])
-        out_v[s] = (projected * lax.rsqrt(square + NORM_FLOOR)).astype(BF16)
-        pltpu.make_async_copy(out_v.at[s], out.at[s], out_sem.at[s]).start()
+        out[s] = (projected * lax.rsqrt(square + NORM_FLOOR)).astype(BF16)
         mine, theirs = lnat[s, core], lrx[s]
         upper = jnp.where(core == 0, mine, theirs)
         lower = jnp.where(core == 0, theirs, mine)
@@ -459,9 +459,18 @@
         for copy in x_sends(s, 0) + x_sends(s, 1):
             copy.wait_send()
         log_send(s).wait_send()
-        pltpu.make_async_copy(out_v.at[s], out.at[s], out_sem.at[s]).wait()
         return 0
     lax.fori_loop(0, seqs, drain, 0)
+
+
+def hand_over(mixed, logs, out, out_logs, sem):
+    seqs = mixed.shape[0]
+    copies = [pltpu.make_async_copy(mixed.at[s], out.at[s], sem.at[s]) for s in range(seqs)]
+    copies.append(pltpu.make_async_copy(logs, out_logs, sem.at[seqs]))
+    for copy in copies:
+        copy.start()
+    for copy in copies:
+        copy.wait()
 
 
 def shards(chips, tps, tokens, query_weight, key_weight, value_weight, out_gain, out_weight):
@@ -471,12 +480,12 @@
     vmem = pl.BlockSpec(memory_space=pltpu.VMEM)
     dma = pltpu.SemaphoreType.DMA
     grid4 = (OWN, 4, 4, 16, HEAD_DIM)
-    return pl.pallas_call(
+    mixed, logs = pl.pallas_call(
         functools.partial(kernel, chips, tps, seqs),
         out_shape=(pltpu.VMEM((seqs, length, out_cols), BF16),
-                   jax.ShapeDtypeStruct((seqs, 2, length), F32)),
+                   pltpu.VMEM((seqs, 2, length), F32)),
         in_specs=[any_spec] * 6,
-        out_specs=(any_spec, vmem),
+        out_specs=(vmem, vmem),
         scratch_shapes=[
             pltpu.VMEM((TOK, HEAD_DIM), F32),
             pltpu.VMEM((TOK, HEAD_DIM), F32),
@@ -505,7 +514,6 @@
             pltpu.VMEM((seqs, 2, 3, 128), F32),
             pltpu.VMEM((seqs, 3, 128), F32),
             pltpu.VMEM((seqs, TOK, channels), BF16),
-            pltpu.VMEM((seqs, TOK, out_cols), BF16),
             dma((7 + seqs,)),
             dma((seqs, 2)),
             dma((seqs, 12)),
@@ -515,12 +523,19 @@
             dma((seqs,)),
             dma((seqs,)),
             dma((seqs,)),
-            dma((seqs,)),
         ],
         compiler_params=pltpu.CompilerParams(
             collective_id=0, has_side_effects=True, vmem_limit_bytes=62 * 1024 * 1024
         ),
     )(tokens, query_weight, key_weight, value_weight, out_gain.reshape(1, channels), out_weight)
+    return pl.pallas_call(
+        hand_over,
+        out_shape=(jax.ShapeDtypeStruct(mixed.shape, BF16), jax.ShapeDtypeStruct(logs.shape, F32)),
+        in_specs=[vmem, vmem],
+        out_specs=(any_spec, any_spec),
+        scratch_shapes=[dma((seqs + 1,))],
+        compiler_params=pltpu.CompilerParams(vmem_limit_bytes=HAND_OVER),
+    )(mixed, logs)
 
 
 def solution(mesh):

time: 73 us -> 71.4 us (0.978)
  local copies, waits for them, and re-layouts: 1.75 us -> 0 us
    unnamed x4 -> x0, local copies, waits for them, and re-layouts: 1.75 us -> none
    pallas_call x0 -> x1, Pallas kernels: none -> 1.18 us  [shards(): pl.pallas_call(hand_over, out_shape=(jax.ShapeDtypeStruct(mixed.shape, BF...]
    pallas_call x1, Pallas kernels: 70.5 us -> 69.5 us  [shards(): pl.pallas_call(functools.partial(kernel, chips, tps, seqs), out_shape=(pl...]
where the time goes in v6:
time: 71.4 us; the launch traced here: 71.3 us
  Pallas kernels  70.7 us (99%)
    pallas_call x1, Pallas kernels, shards(): pl.pallas_call(functools.partial(kernel, chips, tps, seqs), out_shape=(pl...  69.5 us

profile of v6, /device:TPU:193, one launch (start us, length us, event | category | flops | bytes accessed | tf_op | source)
XLA Modules:
  0.0 71.3 jit_solution(15215480381168687389)
XLA Ops:
  0.6 69.5 %shard_map.77 = (bf16[4,384,512]{2,1,0:T(8,128)(2,1)S(1)}, f32[4,2,384]{2,1,0:T(2,128)S(1)}) custom-call(bf16[4,384,2048]{2,1,0:T(8,128)(2,1)} %tokens.1, bf16[2048,256]{1,0:T(8,128)(2,1)} %wq.1, bf16[2048,256]{1,0:T(8,128)(2,1)} %wk.1, bf16[2048,256]{1,0:T(8,128)(2,1)} %wv.1, f32[1,1024]{1,0:T(1,128)} %bitcast.1, bf16[1024,512]{1,0:T(8,128)(2,1)} %wo.1), custom_call_target="tpu_custom_call" | custom-call | tf_op jit(solution)/shard_map/pallas_call | solution.py:483
  70.1 1.2 %shard_map.78 = (bf16[4,384,512]{2,1,0:T(8,128)(2,1)}, f32[4,2,384]{2,1,0:T(2,128)}) custom-call(bf16[4,384,512]{2,1,0:T(8,128)(2,1)S(1)} %get-tuple-element.4.mixed, f32[4,2,384]{2,1,0:T(2,128)S(1)} %get-tuple-element.5.logs), custom_call_target="tpu_custom_call" | custom-call | tf_op jit(solution)/shard_map/pallas_call | solution.py:531

commit v7 on v6

--- a/solution.py
+++ b/solution.py
@@ -196,14 +196,13 @@
     def x_local(s):
         return pltpu.make_async_copy(mnat.at[s, row_of(TOK * core, TOK)], mg.at[s, :, column_of(head)], x_loc.at[s])
 
-    def x_arrivals(s):
+    def x_arrivals(s, piece):
         waits = []
-        for piece in range(2):
-            at, size = piece_of(piece, core)
-            for o in range(1, 2 * tps):
-                other = (head + o) % (2 * tps)
-                waits.append(remote(mnat.at[s, pl.ds(0, size)], mg.at[s, row_of(at, size), column_of(other)],
-                                    x_send.at[s, 0], x_recv.at[s, 8 * piece + other], (2 * chip + 1 - core, tp)))
+        at, size = piece_of(piece, core)
+        for o in range(1, 2 * tps):
+            other = (head + o) % (2 * tps)
+            waits.append(remote(mnat.at[s, pl.ds(0, size)], mg.at[s, row_of(at, size), column_of(other)],
+                                x_send.at[s, 0], x_recv.at[s, 8 * piece + other], (2 * chip + 1 - core, tp)))
         return waits
 
     def turned(x):
@@ -380,14 +379,17 @@
 
     def finish(s):
         x_local(s).wait()
-        for copy in x_arrivals(s):
-            copy.wait_recv()
+        for piece in range(2):
+            for copy in x_arrivals(s, piece):
+                copy.wait_recv()
+            at, size = piece_of(piece, core)
+            rows = row_of(at, size)
+            lifted = mg[s, rows, :].astype(F32)
+            square = jnp.mean(lifted * lifted, axis=-1, keepdims=True)
+            scaled = (lifted * gain[...]).astype(BF16)
+            projected = dot(scaled, wo_v[...])
+            out[s, rows, :] = (projected * lax.rsqrt(square + NORM_FLOOR)).astype(BF16)
         log_send(s).wait_recv()
-        lifted = mg[s].astype(F32)
-        square = jnp.mean(lifted * lifted, axis=-1, keepdims=True)
-        scaled = (lifted * gain[...]).astype(BF16)
-        projected = dot(scaled, wo_v[...])
-        out[s] = (projected * lax.rsqrt(square + NORM_FLOOR)).astype(BF16)
         mine, theirs = lnat[s, core], lrx[s]
         upper = jnp.where(core == 0, mine, theirs)
         lower = jnp.where(core == 0, theirs, mine)
@@ -415,9 +417,10 @@
             def _():
                 far_send(s, way).start()
 
-        @pl.when(s + 1 < seqs)
-        def _():
-            start_near(s + 1)
+            @pl.when(jnp.logical_and(sends_to[way], s + 1 < seqs))
+            def _():
+                for copy in near_sends(s + 1, way):
+                    copy.start()
 
         for copy in local_copies(s):
             copy.wait()

time: 71.4 us -> 71.3 us (level)
  no operation moved by 1% of the time
where the time goes in v7:
time: 71.3 us; the launch traced here: 71.2 us
  Pallas kernels  70.6 us (99%)
    pallas_call x1, Pallas kernels, shards(): pl.pallas_call(functools.partial(kernel, chips, tps, seqs), out_shape=(pl...  69.4 us

profile of v7, /device:TPU:193, one launch (start us, length us, event | category | flops | bytes accessed | tf_op | source)
XLA Modules:
  0.0 71.2 jit_solution(5349706202919823663)
XLA Ops:
  0.6 69.4 %shard_map.77 = (bf16[4,384,512]{2,1,0:T(8,128)(2,1)S(1)}, f32[4,2,384]{2,1,0:T(2,128)S(1)}) custom-call(bf16[4,384,2048]{2,1,0:T(8,128)(2,1)} %tokens.1, bf16[2048,256]{1,0:T(8,128)(2,1)} %wq.1, bf16[2048,256]{1,0:T(8,128)(2,1)} %wk.1, bf16[2048,256]{1,0:T(8,128)(2,1)} %wv.1, f32[1,1024]{1,0:T(1,128)} %bitcast.1, bf16[1024,512]{1,0:T(8,128)(2,1)} %wo.1), custom_call_target="tpu_custom_call" | custom-call | tf_op jit(solution)/shard_map/pallas_call | solution.py:486
  70.0 1.2 %shard_map.78 = (bf16[4,384,512]{2,1,0:T(8,128)(2,1)}, f32[4,2,384]{2,1,0:T(2,128)}) custom-call(bf16[4,384,512]{2,1,0:T(8,128)(2,1)S(1)} %get-tuple-element.4.mixed, f32[4,2,384]{2,1,0:T(2,128)S(1)} %get-tuple-element.5.logs), custom_call_target="tpu_custom_call" | custom-call | tf_op jit(solution)/shard_map/pallas_call | solution.py:534

commit v8 on v7

--- a/solution.py
+++ b/solution.py
@@ -265,7 +265,8 @@
         at = first + (b + col // 64 - 1) * BLK
         good = (gap >= -REACH) & (gap <= REACH) & (at >= 0) & (at < limit)
         bias4[b] = jnp.where(good, 0.0, MASK_FILL)
-    for ref, q_blocks, k_blocks in ((bias_mid, (1,), range(1, NBLK - 1)), (bias_out, (0, 2), range(NBLK))):
+    for ref, q_blocks, k_blocks in ((bias_mid, (1,), range(1, NBLK - 1)), (bias_out.at[0], (0,), range(NBLK - 2)),
+                                   (bias_out.at[1], (2,), range(2, NBLK))):
         dims = (16 * len(q_blocks), 16 * len(k_blocks))
         row, col = iota(dims, 0), iota(dims, 1)
         q_at = row % 16 + 16 * (q_blocks[0] + 2 * (row // 16))
@@ -362,11 +363,14 @@
 
     def far(s):
         put_in_order(s, (0, NBLK - 1))
-        pipelined([wide(r, (0, 2), range(NBLK), bias_out) for r in range(4)])
-        for b in (0, 2):
+        sends = x_sends(s, 1)
+        for half in range(2):
+            b = 2 * half
+            pipelined([wide(r, (b,), range(b, b + NBLK - 2), bias_out.at[half]) for r in range(4)])
             in_order(s, b)
-        for copy in x_sends(s, 1):
-            copy.start()
+            for copy in sends[half:-1:2]:
+                copy.start()
+        sends[-1].start()
         x_local(s).start()
         for b in range(OWN):
             column = lperm[b].reshape(BLK, HEAD_DIM)
@@ -507,7 +511,7 @@
             pltpu.VMEM((OWN, BLK, BLK + 2 * REACH), F32),
             pltpu.VMEM((OWN, 64, 192), F32),
             pltpu.VMEM((16, 16 * (NBLK - 2)), F32),
-            pltpu.VMEM((32, 16 * NBLK), F32),
+            pltpu.VMEM((2, 16, 16 * (NBLK - 2)), F32),
             pltpu.VMEM(grid4, F32),
             pltpu.VMEM(grid4, F32),
             pltpu.VMEM(grid4, F32),

time: 71.3 us -> 71.3 us (level)
  no operation moved by 1% of the time
where the time goes in v8:
time: 71.3 us; the launch traced here: 71.2 us
  Pallas kernels  70.6 us (99%)
    pallas_call x1, Pallas kernels, shards(): pl.pallas_call(functools.partial(kernel, chips, tps, seqs), out_shape=(pl...  69.4 us

profile of v8, /device:TPU:193, one launch (start us, length us, event | category | flops | bytes accessed | tf_op | source)
XLA Modules:
  0.0 71.2 jit_solution(17251226307470923563)
XLA Ops:
  0.6 69.4 %shard_map.77 = (bf16[4,384,512]{2,1,0:T(8,128)(2,1)S(1)}, f32[4,2,384]{2,1,0:T(2,128)S(1)}) custom-call(bf16[4,384,2048]{2,1,0:T(8,128)(2,1)} %tokens.1, bf16[2048,256]{1,0:T(8,128)(2,1)} %wq.1, bf16[2048,256]{1,0:T(8,128)(2,1)} %wk.1, bf16[2048,256]{1,0:T(8,128)(2,1)} %wv.1, f32[1,1024]{1,0:T(1,128)} %bitcast.1, bf16[1024,512]{1,0:T(8,128)(2,1)} %wo.1), custom_call_target="tpu_custom_call" | custom-call | tf_op jit(solution)/shard_map/pallas_call | solution.py:490
  70.0 1.2 %shard_map.78 = (bf16[4,384,512]{2,1,0:T(8,128)(2,1)}, f32[4,2,384]{2,1,0:T(2,128)}) custom-call(bf16[4,384,512]{2,1,0:T(8,128)(2,1)S(1)} %get-tuple-element.4.mixed, f32[4,2,384]{2,1,0:T(2,128)S(1)} %get-tuple-element.5.logs), custom_call_target="tpu_custom_call" | custom-call | tf_op jit(solution)/shard_map/pallas_call | solution.py:538
